TPU v7x, 256 devices: a whole 4x4x8 slice. The times are simulated.
256 devices in a mesh: ep: 64 (over z, y, core), tp: 4 (over x).
Axes of the slice: x: 4, y: 4, z: 8, core: 2. Of those that a mesh axis runs over, the one named last changes fastest.
Arguments:
- queries: bfloat16 [16384, 768], P('ep', 'tp'), may hold values from -270 to 270
- key_rows: bfloat16 [16384, 256], P('ep', 'tp'), may hold values from -6 to 6
- value_rows: bfloat16 [16384, 256], P('ep', 'tp'), may hold values from -6 to 6
- sink_logits: float32 [12], P('tp'), may hold values from 2 to 6
- out_weight: bfloat16 [768, 2048], P('tp'), may hold values from -0.21875 to 0.21875
- mix_gain: float32 [2048], replicated, may hold values from 0.1 to 1.9
- moe_tokens: bfloat16 [32768, 2048], P(('ep', 'tp')), may hold values from -600 to 600
- moe_gain: float32 [2048], replicated, may hold values from 0.1 to 1.9
- routes: int32 [32768, 2], P(('ep', 'tp')), may hold values from 0 to 63, all different within a row; in each aligned block of 128 rows (0 to 127, 128 to 255, ...) at most 5 rows name the same one
- route_weights: float32 [32768, 2], P(('ep', 'tp')), may hold values from 0.25 to 1.5
- expert_gate: bfloat16 [64, 2048, 3584], P('ep', None, 'tp'), may hold values from -0.125 to 0.125
- expert_up: bfloat16 [64, 2048, 3584], P('ep', None, 'tp'), may hold values from -0.125 to 0.125
- expert_down: bfloat16 [64, 3584, 2048], P('ep', 'tp'), may hold values from -0.09375 to 0.09375
Outputs:
- mixed: bfloat16 [16384, 2048], P(('ep', 'tp'))
- moe_out: bfloat16 [32768, 2048], P(('ep', 'tp'))
Inputs may be any that keep to these rules, and one draw needn't show every extreme that they name: `routes`: each row names 2 different experts. In the rows of one device no expert is named more than 5 times, and in every draw some device names some expert exactly 5 times.
All inputs are finite; a program needn't handle non-finite values.
Results may differ from a plain program's by a relative error of at most 0.012.
Values may be sent and summed in bfloat16 or wider, within the bound.
A program may use at most 128 MiB of HBM per device.

v0:
```python
import jax
import jax.numpy as jnp
from jax import lax
from jax.sharding import PartitionSpec as P

HDIM = 64
WINDOW = 128


norm_eps = 1e-06
masked_value = -1e30


def shifted(shard, axis, by):
    size = lax.axis_size(axis)
    pairs = [(i, i + by) for i in range(size) if 0 <= i + by < size]
    return lax.ppermute(shard, axis, pairs)


def rms_scale(rows_in, gain):
    squares = jnp.mean(rows_in * rows_in, axis=-1, keepdims=True)
    return rows_in * lax.rsqrt(squares + norm_eps) * gain


def mixer(queries, key_rows, value_rows, sink_logits, out_weight, mix_gain):
    tok_rows = queries.shape[0]
    kv_local = key_rows.shape[1] // HDIM
    group_size = queries.shape[1] // key_rows.shape[1]
    rim_rows = (key_rows[tok_rows - WINDOW :], value_rows[tok_rows - WINDOW :])
    prev_keys, prev_values = shifted((rim_rows[0], rim_rows[1]), "ep", 1)
    all_keys = jnp.concatenate([prev_keys, key_rows], axis=0).reshape(
        tok_rows + WINDOW, kv_local, HDIM
    )
    all_values = jnp.concatenate([prev_values, value_rows], axis=0).reshape(
        tok_rows + WINDOW, kv_local, HDIM
    )
    offset = lax.axis_index("ep") * tok_rows
    query_pos = offset + jnp.arange(tok_rows, dtype=jnp.int32)
    key_pos = offset - WINDOW + jnp.arange(tok_rows + WINDOW, dtype=jnp.int32)
    distance = query_pos[:, None] - key_pos[None, :]
    allowed = (distance >= 0) & (distance < WINDOW) & (key_pos >= 0)[None, :]
    grouped = queries.reshape(tok_rows, kv_local, group_size, HDIM)
    scores = jnp.einsum(
        "qkgd,jkd->kgqj", grouped, all_keys, preferred_element_type=jnp.float32
    ) * HDIM ** (-0.5)
    logits = jnp.where(allowed, scores, masked_value)
    sink_logit = sink_logits.reshape(kv_local, group_size)[:, :, None, None]
    top_value = jnp.maximum(jnp.max(logits, axis=-1, keepdims=True), sink_logit)
    exponent = jnp.exp(logits - top_value)
    denominator = jnp.sum(exponent, axis=-1, keepdims=True) + jnp.exp(sink_logit - top_value)
    probs = (exponent / denominator).astype(jnp.bfloat16)
    attended = jnp.einsum("kgqj,jkd->qkgd", probs, all_values, preferred_element_type=jnp.float32)
    attended = attended.astype(jnp.bfloat16).reshape(tok_rows, -1)
    projected = lax.psum_scatter(
        jnp.dot(attended, out_weight, preferred_element_type=jnp.float32).astype(jnp.bfloat16),
        "tp",
        scatter_dimension=0,
        tiled=True,
    ).astype(jnp.float32)
    return rms_scale(projected, mix_gain).astype(jnp.bfloat16)


def slot_places(route_rows, experts):
    blocks, tok_rows, top_count = route_rows.shape
    flat_routes = route_rows.reshape(blocks, tok_rows * top_count)
    onehot = (
        flat_routes[:, :, None] == jnp.arange(experts, dtype=jnp.int32)[None, None, :]
    ).astype(jnp.int32)
    earlier = jnp.cumsum(onehot, axis=1) - onehot
    slot_rank = jnp.sum(earlier * onehot, axis=2)
    return (slot_rank * experts + flat_routes).reshape(blocks, tok_rows, top_count)


def dispatch_matrix(slot_place, slots):
    targets = jnp.arange(slots, dtype=jnp.int32)
    hits = (slot_place[:, None, :, :] == targets[None, :, None, None]).astype(jnp.float32)
    return jnp.sum(hits, axis=3).astype(jnp.bfloat16)


def routed_experts(
    moe_tokens, moe_gain, routes, route_weights, expert_gate, expert_up, expert_down
):
    tok_rows, width = moe_tokens.shape
    top_count = routes.shape[1]
    experts = lax.axis_size("ep")
    capacity = tok_rows * top_count * 5 // (4 * experts)
    normed = rms_scale(moe_tokens.astype(jnp.float32), moe_gain).astype(jnp.bfloat16)
    gate_weight = expert_gate[0]
    up_weight = expert_up[0]
    down_weight = expert_down[0]
    slot_place = slot_places(routes[None], experts)
    select_rows = dispatch_matrix(slot_place, capacity * experts)[0]
    outgoing = jnp.dot(select_rows, normed, preferred_element_type=jnp.float32)
    outgoing = outgoing.astype(jnp.bfloat16).reshape(capacity, experts, width)
    slot_rows = lax.all_gather(
        lax.all_to_all(outgoing, "ep", split_axis=1, concat_axis=1, tiled=True),
        "tp",
        axis=0,
        tiled=True,
    )
    gate_value = jnp.dot(slot_rows, gate_weight, preferred_element_type=jnp.float32)
    up_value = jnp.dot(slot_rows, up_weight, preferred_element_type=jnp.float32)
    hidden = (jax.nn.silu(gate_value) * up_value).astype(jnp.bfloat16)
    summed = lax.psum_scatter(
        jnp.dot(hidden, down_weight, preferred_element_type=jnp.float32).astype(jnp.bfloat16),
        "tp",
        scatter_dimension=0,
        tiled=True,
    )
    returned = lax.all_to_all(summed, "ep", split_axis=1, concat_axis=1, tiled=True)
    flat_returned = returned.reshape(capacity * experts, width)
    picked = flat_returned[slot_place[0]]
    combined = jnp.sum(route_weights[:, :, None] * picked.astype(jnp.float32), axis=1)
    return combined.astype(jnp.bfloat16)


def shards(
    queries,
    key_rows,
    value_rows,
    sink_logits,
    out_weight,
    mix_gain,
    moe_tokens,
    moe_gain,
    routes,
    route_weights,
    expert_gate,
    expert_up,
    expert_down,
):
    mixed = mixer(queries, key_rows, value_rows, sink_logits, out_weight, mix_gain)
    moe_out = routed_experts(
        moe_tokens, moe_gain, routes, route_weights, expert_gate, expert_up, expert_down
    )
    return (mixed, moe_out)


def solution(mesh):
    return jax.shard_map(
        shards,
        mesh=mesh,
        in_specs=(
            P("ep", "tp"),
            P("ep", "tp"),
            P("ep", "tp"),
            P("tp"),
            P("tp", None),
            P(),
            P(("ep", "tp"), None),
            P(),
            P(("ep", "tp"), None),
            P(("ep", "tp"), None),
            P("ep", None, "tp"),
            P("ep", None, "tp"),
            P("ep", "tp", None),
        ),
        out_specs=(P(("ep", "tp"), None), P(("ep", "tp"), None)),
        check_vma=False,
    )
```

profile of v0, /device:TPU:1, one launch (start us, length us, event | category | flops | bytes accessed | tf_op | source)
XLA Modules:
  0.0 303.0 jit_solution(3344999738378034073)
XLA Ops:
  7.2 0.0 all-gather.2.cloned.1.call-start
  7.2 0.8 copy.38
  8.1 0.1 eq.48
  8.2 0.1 compare_convert_fusion
  8.3 0.6 reduce-window.6
  8.9 0.2 slice_reduce_fusion
  9.1 0.1 copy.40
  9.2 0.1 copy.41
  9.3 0.1 broadcast.151
  9.4 0.1 fusion.25
  9.6 0.1 mul.99
  9.7 0.1 copy.43
  9.8 0.1 convert_reduce_fusion
  9.9 1.2 fusion.9
  11.1 1.6 convolution_convert_fusion.1
  12.8 0.7 copy.44
  13.5 62.6 %all_to_all.10 = bf16[5,64,2048]{2,0,1:T(8,128)(2,1)S(1)} all-to-all(bf16[5,64,2048]{2,0,1:T(8,128)(2,1)S(1)} %copy.44), channel_id=1, replica_groups=mesh['ep'=64,'tp'=4] {'ep'}, dimensions={1} | all-to-all | bytes 2621440 | tf_op jit(solution)/shard_map/all_to_all | solution.py:96
  76.2 1.9 copy.45
  78.1 0.0 all-gather.2.cloned.1.call-update
  78.1 0.0 reduce-scatter.5.cloned.1.call-start
  78.1 57.0 %all-gather.2.cloned.1.call-done = bf16[20,64,2048]{2,1,0:T(8,128)(2,1)} async-done(((bf16[5,64,2048]{2,1,0:T(8,128)(2,1)}), bf16[20,64,2048]{2,1,0:T(8,128)(2,1)}) %all-gather.2.cloned.1.call-update) | async-done | bytes 5242896 | tf_op jit(solution)/shard_map/all_gather | solution.py:95
  135.1 10.0 %fusion.1 = f32[20,64,896]{2,1,0:T(8,128)} fusion(bf16[20,64,2048]{2,1,0:T(8,128)(2,1)} %all-gather.2.cloned.1.call-done, bf16[1,2048,896]{2,1,0:T(8,128)(2,1)} %param.24), kind=kOutput, calls=%fused_computation.4 | convolution fusion | flops 4697620480 | bytes 13500416 | tf_op jit(solution)/shard_map/dot_general | solution.py:102
  145.1 17.5 %convolution_convert_fusion = bf16[20,64,2048]{2,1,0:T(8,128)(2,1)} fusion(bf16[1,896,2048]{2,1,0:T(8,128)(2,1)} %param.25, f32[20,64,896]{2,1,0:T(8,128)} %fusion.1, bf16[20,64,2048]{2,1,0:T(8,128)(2,1)} %all-gather.2.cloned.1.call-done, bf16[1,2048,896]{2,1,0:T(8,128)(2,1)} %param.23), kind=kOutput, calls=%fused_computation.2 | convolution fusion | flops 9404743680 | bytes 22413312 | tf_op jit(solution)/shard_map/dot_general | solution.py:105
  162.7 0.0 reduce-scatter.5.cloned.1.call-update
  162.7 0.0 reduce-scatter.3.cloned.1.call-start
  162.7 0.7 copy-done.2
  163.4 3.8 %collective-permute-start.1 = (bf16[128,64]{0,1:T(8,128)(2,1)S(1)}, bf16[128,64]{0,1:T(8,128)(2,1)S(1)}, u32[]{:S(2)}, u32[]{:S(2)}) collective-permute-start(bf16[128,64]{0,1:T(8,128)(2,1)S(1)} %slice.13), channel_id=1, source_target_pairs={{0,4},{4,8},{8,12},{12,16},{16,20},{20,24},{24,28},{28,32},{32,36}... | collective-permute-start | bytes 49160 | tf_op jit(solution)/shard_map/ppermute | solution.py:17
  167.3 2.1 collective-permute-start
  169.4 0.2 fusion.23
  169.6 0.4 fusion.33
  170.0 0.1 broadcast_maximum_fusion
  170.1 0.2 fusion.12
  170.2 0.1 exponential_add_fusion
  170.3 0.3 convolution_convert_fusion.3
  170.7 1.5 convolution_convert_fusion.2
  172.2 49.2 %reduce-scatter.5.cloned.1.call-done = bf16[5,64,2048]{2,1,0:T(8,128)(2,1)} async-done(((bf16[20,64,2048]{2,1,0:T(8,128)(2,1)}), bf16[5,64,2048]{2,1,0:T(8,128)(2,1)}) %reduce-scatter.5.cloned.1.call-update) | async-done | bytes 1310736 | tf_op jit(solution)/shard_map/reduce_scatter | solution.py:104
  221.4 3.4 %copy.46 = bf16[5,64,2048]{2,0,1:T(8,128)(2,1)} copy(bf16[5,64,2048]{2,1,0:T(8,128)(2,1)} %reduce-scatter.5.cloned.1.call-done) | data formatting | bytes 2621440 | tf_op jit(solution)/shard_map/reduce_scatter | solution.py:104
  224.8 11.0 %all-to-all-start.1 = ((bf16[5,64,2048]{2,0,1:T(8,128)(2,1)}), bf16[5,64,2048]{2,0,1:T(8,128)(2,1)}, u32[]{:S(2)}, u32[]{:S(2)}) async-start(bf16[5,64,2048]{2,0,1:T(8,128)(2,1)} %copy.46), calls=%async_computation.3 | async-start | bytes 4194304 | tf_op jit(solution)/shard_map/all_to_all | solution.py:110
  235.8 0.1 reshape.289
  235.9 0.1 copy.37
  236.1 12.6 %reduce-scatter.3.cloned.1.call-done = bf16[64,2048]{1,0:T(8,128)(2,1)} async-done(((bf16[256,2048]{1,0:T(8,128)(2,1)}), bf16[64,2048]{1,0:T(8,128)(2,1)}) %reduce-scatter.3.cloned.1.call-update) | async-done | bytes 262160 | tf_op jit(solution)/shard_map/reduce_scatter | solution.py:54
  248.6 1.1 fusion.16
  249.7 1.8 fusion.18
  251.5 33.9 %all-to-all-done.1 = bf16[5,64,2048]{2,0,1:T(8,128)(2,1)} async-done(((bf16[5,64,2048]{2,0,1:T(8,128)(2,1)}), bf16[5,64,2048]{2,0,1:T(8,128)(2,1)}, u32[]{:S(2)}, u32[]{:S(2)}) %all-to-all-start.1) | async-done | bytes 1310752 | tf_op jit(solution)/shard_map/all_to_all | solution.py:110
  285.4 2.4 copy.47
  287.9 2.3 gather_fusion
  290.2 2.4 reshape.297
  292.6 3.9 %multiply_reduce_fusion = bf16[128,2048]{1,0:T(8,128)(2,1)} fusion(f32[128,2,2048]{2,1,0:T(2,128)S(1)} %reshape.297, f32[128,2]{1,0:T(8,128)S(1)} %copy.37), kind=kLoop, calls=%fused_computation.10 | loop fusion | flops 786432 | bytes 2622464 | tf_op jit(solution)/shard_map/reduce_sum | solution.py:113
  (29 shorter events, 0.2 us)
Async XLA Ops:
  7.2 163.5 %copy-start = (bf16[192,2048]{1,0:T(8,128)(2,1)S(1)}, bf16[192,2048]{1,0:T(8,128)(2,1)}, u32[]{:S(2)}) copy-start(bf16[192,2048]{1,0:T(8,128)(2,1)} %param.17) | copy-start | bytes 2359300
  7.2 128.0 %all-gather.2.cloned.1.call-start = ((), (), s32[]{:S(2)}) async-start(), calls=%async_computation.5 | async-start | bytes 6553600 | tf_op jit(solution)/shard_map/all_gather | solution.py:95
  78.1 143.3 %reduce-scatter.5.cloned.1.call-start = ((), (), s32[]{:S(2)}) async-start(), calls=%async_computation.6 | async-start | bytes 6553600 | tf_op jit(solution)/shard_map/reduce_scatter | solution.py:104
  162.6 0.8 copy-start.2
  162.6 4.6 %copy-start.3 = (bf16[256,64]{0,1:T(8,128)(2,1)S(1)}, bf16[256,64]{0,1:T(8,128)(2,1)}, u32[]{:S(2)}) copy-start(bf16[256,64]{0,1:T(8,128)(2,1)} %param.15) | copy-start | bytes 98308
  162.6 7.0 %copy-start.6 = (bf16[256,192]{0,1:T(8,128)(2,1)S(1)}, bf16[256,192]{0,1:T(8,128)(2,1)}, u32[]{:S(2)}) copy-start(bf16[256,192]{0,1:T(8,128)(2,1)} %param.13) | copy-start | bytes 294916
  162.6 7.3 %copy-start.4 = (f32[3]{0:T(128)S(1)}, f32[3]{0:T(128)}, u32[]{:S(2)}) copy-start(f32[3]{0:T(128)} %param.16) | copy-start | bytes 40
  162.7 85.9 %reduce-scatter.3.cloned.1.call-start = ((), (), s32[]{:S(2)}) async-start(), calls=%async_computation.4 | async-start | bytes 1310720 | tf_op jit(solution)/shard_map/reduce_scatter | solution.py:54
  163.4 6.2 %collective-permute-start.1 = (bf16[128,64]{0,1:T(8,128)(2,1)S(1)}, bf16[128,64]{0,1:T(8,128)(2,1)S(1)}, u32[]{:S(2)}, u32[]{:S(2)}) collective-permute-start(bf16[128,64]{0,1:T(8,128)(2,1)S(1)} %slice.13), channel_id=1, source_target_pairs={{0,4},{4,8},{8,12},{12,16},{16,20},{20,24},{24,28},{28,32},{32,36}... | collective-permute-start | bytes 49160 | tf_op jit(solution)/shard_map/ppermute | solution.py:17
  167.3 3.1 %collective-permute-start = (bf16[128,64]{0,1:T(8,128)(2,1)S(1)}, bf16[128,64]{0,1:T(8,128)(2,1)S(1)}, u32[]{:S(2)}, u32[]{:S(2)}) collective-permute-start(bf16[128,64]{0,1:T(8,128)(2,1)S(1)} %slice.12), channel_id=1, source_target_pairs={{0,4},{4,8},{8,12},{12,16},{16,20},{20,24},{24,28},{28,32},{32,36}... | collective-permute-start | bytes 49160 | tf_op jit(solution)/shard_map/ppermute | solution.py:17
  172.2 63.8 %copy-start.5 = (f32[128,2]{0,1:T(2,128)S(1)}, f32[128,2]{0,1:T(2,128)}, u32[]{:S(2)}) copy-start(f32[128,2]{0,1:T(2,128)} %param.22) | copy-start | bytes 3076
  172.2 77.6 %copy-start.1 = (f32[2048]{0:T(1024)S(1)}, f32[2048]{0:T(1024)}, u32[]{:S(2)}) copy-start(f32[2048]{0:T(1024)} %param.18) | copy-start | bytes 24580
  224.8 60.6 %all-to-all-start.1 = ((bf16[5,64,2048]{2,0,1:T(8,128)(2,1)}), bf16[5,64,2048]{2,0,1:T(8,128)(2,1)}, u32[]{:S(2)}, u32[]{:S(2)}) async-start(bf16[5,64,2048]{2,0,1:T(8,128)(2,1)} %copy.46), calls=%async_computation.3 | async-start | bytes 4194304 | tf_op jit(solution)/shard_map/all_to_all | solution.py:110
Sparse Core Ops, SparseCore 0:
  78.2 56.8 all-gather.1
  162.8 58.5 reduce-scatter.4
  224.0 24.6 reduce-scatter.2
where the time goes:
time: 304 us; the launch traced here: 303 us
  waiting for transfers between devices  153 us (50%)
  blocking collectives  62.6 us (21%)
  matrix products  31.3 us (10%)
  starting transfers between devices  17 us (6%)
  local copies, waits for them, and re-layouts  15.9 us (5%)
  between operations  14 us (5%)
  other arithmetic  9.51 us (3%)
    all_to_all x1, blocking collectives, routed_experts(): lax.all_to_all(outgoing, 'ep', split_axis=1, concat_axis=1, tiled=True)  62.6 us
    all_gather x1, waiting for transfers between devices, routed_experts(): lax.all_gather(lax.all_to_all(outgoing, 'ep', split_axis=1, concat_axis=1...  57 us
    reduce_scatter x1, waiting for transfers between devices, routed_experts(): lax.psum_scatter(jnp.dot(hidden, down_weight, preferred_element_type=jnp....  49.2 us
    all_to_all x1, waiting for transfers between devices, routed_experts(): lax.all_to_all(summed, 'ep', split_axis=1, concat_axis=1, tiled=True)  33.9 us
    dot_general x1, matrix products, routed_experts(): jnp.dot(hidden, down_weight, preferred_element_type=jnp.float32)  17.5 us
    reduce_scatter x1, waiting for transfers between devices, mixer(): lax.psum_scatter(jnp.dot(attended, out_weight, preferred_element_type=jnp...  12.6 us
    all_to_all x1, starting transfers between devices, routed_experts(): lax.all_to_all(summed, 'ep', split_axis=1, concat_axis=1, tiled=True)  11 us
    dot_general x1, matrix products, routed_experts(): up_value = jnp.dot(slot_rows, up_weight, preferred_element_type=jnp.float32)  10 us
  transfers between devices with their start and end apart: 6, of which 4 were waited for; matrix products, arithmetic and copies ran while one was open for 3% of the time, Pallas kernels for 0%

commit v1 on v0

--- a/solution.py
+++ b/solution.py
@@ -1,14 +1,29 @@
+import functools
+
 import jax
 import jax.numpy as jnp
 from jax import lax
+from jax.experimental import pallas as pl
+from jax.experimental.pallas import tpu as pltpu
 from jax.sharding import PartitionSpec as P
 
 HDIM = 64
 WINDOW = 128
-
+MESH = pl.DeviceIdType.MESH
 
 norm_eps = 1e-06
 masked_value = -1e30
+
+N_Z = 8
+N_YC = 8
+CAP = 5
+CHUNKS = 4
+HALVES = 2
+OFFSETS = ((0, 1), (2, 6), (3, 5), (4, 7))
+SELF_CHUNK = 0
+ROWS = HALVES * N_YC * CAP
+GROUPS = ROWS // 16
+GROUP_ROWS = N_YC * CAP
 
 
 def shifted(shard, axis, by):
@@ -60,58 +75,430 @@
     return rms_scale(projected, mix_gain).astype(jnp.bfloat16)
 
 
-def slot_places(route_rows, experts):
-    blocks, tok_rows, top_count = route_rows.shape
-    flat_routes = route_rows.reshape(blocks, tok_rows * top_count)
-    onehot = (
-        flat_routes[:, :, None] == jnp.arange(experts, dtype=jnp.int32)[None, None, :]
-    ).astype(jnp.int32)
-    earlier = jnp.cumsum(onehot, axis=1) - onehot
-    slot_rank = jnp.sum(earlier * onehot, axis=2)
-    return (slot_rank * experts + flat_routes).reshape(blocks, tok_rows, top_count)
-
-
-def dispatch_matrix(slot_place, slots):
-    targets = jnp.arange(slots, dtype=jnp.int32)
-    hits = (slot_place[:, None, :, :] == targets[None, :, None, None]).astype(jnp.float32)
-    return jnp.sum(hits, axis=3).astype(jnp.bfloat16)
+def pick(index, table):
+    value = jnp.int32(table[-1])
+    for place in range(len(table) - 2, -1, -1):
+        value = jnp.where(index == place, jnp.int32(table[place]), value)
+    return value
+
+
+def rows_to_tiles(block, perm, width):
+    lanes = width // 16
+    stacked = jnp.concatenate(
+        [
+            jnp.concatenate(
+                [block[16 * g : 16 * g + 16, lanes * s : lanes * s + lanes] for s in range(16)],
+                axis=0,
+            )
+            for g in range(GROUPS)
+        ],
+        axis=1,
+    )
+    turned = jnp.dot(perm, stacked, preferred_element_type=jnp.float32).astype(jnp.bfloat16)
+    return [turned[:, lanes * g : lanes * g + lanes].reshape(16, 16, lanes) for g in range(GROUPS)]
+
+
+def tiles_to_rows(tiles, perm, lanes):
+    stacked = jnp.concatenate(
+        [tiles[16 * g : 16 * g + 16].reshape(256, lanes) for g in range(GROUPS)], axis=1
+    )
+    turned = jnp.dot(perm, stacked, preferred_element_type=jnp.float32).astype(jnp.bfloat16)
+    return [
+        [turned[16 * s : 16 * s + 16, lanes * g : lanes * g + lanes] for s in range(16)]
+        for g in range(GROUPS)
+    ]
+
+
+def experts_kernel(
+    n_tp,
+    tokens_ref,
+    gain_ref,
+    routes_ref,
+    weights_ref,
+    gate_ref,
+    up_ref,
+    down_ref,
+    out_ref,
+    outb,
+    recv,
+    xbuf,
+    pbuf,
+    r1,
+    r2,
+    back,
+    ret,
+    wgu,
+    wdn,
+    hid,
+    acc,
+    mix,
+    perm_ref,
+    row_ref,
+    w_sem,
+    a_send,
+    a_recv,
+    g_send,
+    g_recv,
+    q_send,
+    q_recv,
+    b_send,
+    b_recv,
+):
+    width = tokens_ref.shape[1]
+    half = width // 2
+    lanes = width // 16
+    gate_tiles = wgu.shape[0]
+    down_tiles = wdn.shape[0]
+    me = lax.axis_index("ep")
+    tp = lax.axis_index("tp")
+    z = lax.div(me, jnp.int32(N_YC))
+    yc = lax.rem(me, jnp.int32(N_YC))
+    right = lax.rem(tp + 1, jnp.int32(n_tp))
+    left = lax.rem(tp + n_tp - 1, jnp.int32(n_tp))
+
+    barrier = pltpu.get_barrier_semaphore()
+
+    def greet(i, carry):
+        @pl.when(i != me)
+        def _():
+            pl.semaphore_signal(barrier, inc=1, device_id={"ep": i}, device_id_type=MESH)
+
+        return carry
+
+    lax.fori_loop(0, N_Z * N_YC, greet, 0)
+    pl.semaphore_signal(barrier, inc=1, device_id={"tp": right}, device_id_type=MESH)
+    pl.semaphore_signal(barrier, inc=1, device_id={"tp": left}, device_id_type=MESH)
+
+    for n in range(gate_tiles):
+        for part, ref in enumerate((gate_ref, up_ref)):
+            pltpu.make_async_copy(
+                ref.at[0, :, pl.ds(128 * n, 128)], wgu.at[n, :, pl.ds(128 * part, 128)], w_sem.at[0]
+            ).start()
+    for n in range(down_tiles):
+        pltpu.make_async_copy(
+            down_ref.at[0, :, pl.ds(256 * n, 256)], wdn.at[n], w_sem.at[1]
+        ).start()
+
+    tok = tokens_ref.shape[0]
+    e_rows = [routes_ref[0:1, :], routes_ref[1:2, :]]
+    expert_id = lax.broadcasted_iota(jnp.int32, (N_Z * N_YC, tok), 0)
+    named = [jnp.where(expert_id == e, 1.0, 0.0) for e in e_rows]
+    before = jnp.where(
+        lax.broadcasted_iota(jnp.int32, (tok, tok), 0)
+        < lax.broadcasted_iota(jnp.int32, (tok, tok), 1),
+        1.0,
+        0.0,
+    ).astype(jnp.bfloat16)
+    ranks = [
+        jnp.dot(n.astype(jnp.bfloat16), before, preferred_element_type=jnp.float32) for n in named
+    ]
+    ranks[1] = ranks[1] + jnp.sum(named[0], axis=1, keepdims=True)
+    slots = []
+    flat_offsets = [o for pair in OFFSETS for o in pair]
+    for e, n, r in zip(e_rows, named, ranks):
+        rank = jnp.sum(n * r, axis=0, keepdims=True).astype(jnp.int32)
+        offset = (lax.shift_right_logical(e, 3) - z) & (N_Z - 1)
+        place = jnp.zeros_like(offset)
+        for p, o in enumerate(flat_offsets):
+            place = jnp.where(offset == o, p, place)
+        slots.append((place * N_YC + (e & (N_YC - 1))) * CAP + rank)
+
+    i256 = lax.broadcasted_iota(jnp.int32, (256, 256), 0)
+    j256 = lax.broadcasted_iota(jnp.int32, (256, 256), 1)
+    perm_ref[...] = jnp.where(
+        j256 == (i256 & 15) * 16 + lax.shift_right_logical(i256, 4), 1.0, 0.0
+    ).astype(jnp.bfloat16)
+
+    x = tokens_ref[...].astype(jnp.float32)
+    squares = jnp.mean(x * x, axis=-1, keepdims=True)
+    row_ref[...] = (x * lax.rsqrt(squares + norm_eps) * gain_ref[...]).astype(jnp.bfloat16)
+
+    def peer(i, y, sign, k):
+        distance = pick(k, [pair[i] for pair in OFFSETS])
+        return lax.rem(z + sign * distance + N_Z, jnp.int32(N_Z)) * N_YC + y
+
+    def a_copy(k, i, y):
+        return pltpu.make_async_remote_copy(
+            src_ref=outb.at[k, i * N_YC + y],
+            dst_ref=recv.at[k, i * N_YC + yc],
+            send_sem=a_send.at[k],
+            recv_sem=a_recv.at[k],
+            device_id={"ep": peer(i, y, 1, k)},
+            device_id_type=MESH,
+        )
+
+    def b_copy(k, i, y):
+        return pltpu.make_async_remote_copy(
+            src_ref=back.at[k, i * N_YC + y],
+            dst_ref=ret.at[k, i * N_YC + yc],
+            send_sem=b_send.at[k],
+            recv_sem=b_recv.at[k],
+            device_id={"ep": peer(i, y, -1, k)},
+            device_id_type=MESH,
+        )
+
+    def spread(copy_of, k):
+        def one(y, carry):
+            for i in range(HALVES):
+                if i == 0:
+
+                    @pl.when(jnp.logical_not(jnp.logical_and(k == SELF_CHUNK, y == yc)))
+                    def _():
+                        copy_of(k, 0, y).start()
+                else:
+                    copy_of(k, i, y).start()
+            return carry
+
+        lax.fori_loop(0, N_YC, one, 0)
+
+    def bulk(buffer, sem, k):
+        @pl.when(k == SELF_CHUNK)
+        def _():
+            view = buffer.at[k, pl.ds(0, HALVES * N_YC - 1)]
+            pltpu.make_async_copy(view, view, sem.at[k]).wait()
+
+        @pl.when(k != SELF_CHUNK)
+        def _():
+            view = buffer.at[k]
+            pltpu.make_async_copy(view, view, sem.at[k]).wait()
+
+    def dispatch(k, carry):
+        row_id = lax.broadcasted_iota(jnp.int32, (ROWS, tok), 0) + k * ROWS
+        hits = [row_id == s for s in slots]
+        select = jnp.where(jnp.logical_or(hits[0], hits[1]), 1.0, 0.0).astype(jnp.bfloat16)
+        shares = jnp.where(hits[0], weights_ref[0:1, :], 0.0) + jnp.where(
+            hits[1], weights_ref[1:2, :], 0.0
+        )
+        coarse = shares.astype(jnp.bfloat16)
+        mix[k, 0] = coarse
+        mix[k, 1] = (shares - coarse.astype(jnp.float32)).astype(jnp.bfloat16)
+        block = jnp.dot(select, row_ref[...], preferred_element_type=jnp.float32)
+        tiles = rows_to_tiles(block.astype(jnp.bfloat16), perm_ref[...], width)
+        flat = outb.at[k].reshape(ROWS, 16, lanes)
+        for g in range(GROUPS):
+            flat[16 * g : 16 * g + 16] = tiles[g]
+
+        @pl.when(k == 0)
+        def _():
+            pl.semaphore_wait(barrier, N_Z * N_YC - 1 + 2)
+
+        @pl.when(k == SELF_CHUNK)
+        def _():
+            recv[k, yc] = outb[k, yc]
+
+        spread(a_copy, k)
+        return carry
+
+    lax.fori_loop(0, CHUNKS, dispatch, 0)
+    acc[...] = jnp.zeros_like(acc)
+
+    low = pl.ds(0, half)
+    high = pl.ds(half, half)
+
+    def g_copy(k, which):
+        if which == 0:
+            src, dst, to = xbuf.at[k, 0], xbuf.at[k, 1], right
+        elif which == 1:
+            src, dst, to = xbuf.at[k, 0], xbuf.at[k, 2], left
+        elif which == 2:
+            src, dst, to = xbuf.at[k, 1, :, low], xbuf.at[k, 3, :, low], right
+        else:
+            src, dst, to = xbuf.at[k, 2, :, high], xbuf.at[k, 3, :, high], left
+        return pltpu.make_async_remote_copy(
+            src_ref=src,
+            dst_ref=dst,
+            send_sem=g_send.at[k, which],
+            recv_sem=g_recv.at[k, which],
+            device_id={"tp": to},
+            device_id_type=MESH,
+        )
+
+    def q_copy(k, which):
+        if which == 0:
+            src, dst, to = pbuf.at[k, 3, :, low], r1.at[k, 0], right
+        elif which == 1:
+            src, dst, to = pbuf.at[k, 3, :, high], r1.at[k, 1], left
+        elif which == 2:
+            src, dst, to = pbuf.at[k, 2, :, high], r2.at[k, 0, :, high], right
+        elif which == 3:
+            src, dst, to = pbuf.at[k, 1, :, low], r2.at[k, 1, :, low], left
+        elif which == 4:
+            src, dst, to = pbuf.at[k, 2, :, low], r2.at[k, 0, :, low], right
+        else:
+            src, dst, to = pbuf.at[k, 1, :, high], r2.at[k, 1, :, high], left
+        return pltpu.make_async_remote_copy(
+            src_ref=src,
+            dst_ref=dst,
+            send_sem=q_send.at[k, which],
+            recv_sem=q_recv.at[k, which],
+            device_id={"tp": to},
+            device_id_type=MESH,
+        )
+
+    def arrive(k):
+        bulk(recv, a_recv, k)
+        rows = tiles_to_rows(recv[k].reshape(ROWS, 16, lanes), perm_ref[...], lanes)
+        for g in range(GROUPS):
+            for s in range(16):
+                xbuf[k, 0, 16 * g : 16 * g + 16, lanes * s : lanes * s + lanes] = rows[g][s]
+        g_copy(k, 0).start()
+        g_copy(k, 1).start()
+
+    def forward(k):
+        g_copy(k, 0).wait_recv()
+        g_copy(k, 2).start()
+        g_copy(k, 1).wait_recv()
+        g_copy(k, 3).start()
+
+    def multiply(k):
+        @pl.when(k == 0)
+        def _():
+            pltpu.make_async_copy(wgu, wgu, w_sem.at[0]).wait()
+            pltpu.make_async_copy(wdn, wdn, w_sem.at[1]).wait()
+
+        g_copy(k, 2).wait_recv()
+        g_copy(k, 3).wait_recv()
+        for n in range(gate_tiles):
+            both = jnp.dot(
+                xbuf[k].reshape(n_tp * ROWS, width), wgu[n], preferred_element_type=jnp.float32
+            )
+            gate, up = both[:, :128], both[:, 128:]
+            hid[:, 128 * n : 128 * n + 128] = (gate / (1.0 + jnp.exp(-gate)) * up).astype(
+                jnp.bfloat16
+            )
+        for n in range(down_tiles):
+            part = jnp.dot(hid[...], wdn[n], preferred_element_type=jnp.float32)
+            pbuf[k, :, :, 256 * n : 256 * n + 256] = part.astype(jnp.bfloat16).reshape(
+                n_tp, ROWS, 256
+            )
+        for which in range(4):
+            q_copy(k, which).start()
+
+    def relay(k):
+        q_copy(k, 0).wait_recv()
+        pbuf[k, 2, :, low] = (
+            pbuf[k, 2, :, low].astype(jnp.float32) + r1[k, 0].astype(jnp.float32)
+        ).astype(jnp.bfloat16)
+        q_copy(k, 4).start()
+        q_copy(k, 1).wait_recv()
+        pbuf[k, 1, :, high] = (
+            pbuf[k, 1, :, high].astype(jnp.float32) + r1[k, 1].astype(jnp.float32)
+        ).astype(jnp.bfloat16)
+        q_copy(k, 5).start()
+
+    def finish(k):
+        for which in range(2, 6):
+            q_copy(k, which).wait_recv()
+        total = (
+            pbuf[k, 0].astype(jnp.float32)
+            + r2[k, 0].astype(jnp.float32)
+            + r2[k, 1].astype(jnp.float32)
+        ).astype(jnp.bfloat16)
+        tiles = rows_to_tiles(total, perm_ref[...], width)
+        flat = back.at[k].reshape(ROWS, 16, lanes)
+        for g in range(GROUPS):
+            flat[16 * g : 16 * g + 16] = tiles[g]
+
+        @pl.when(k == SELF_CHUNK)
+        def _():
+            ret[k, yc] = back[k, yc]
+
+        spread(b_copy, k)
+
+    def combine(k):
+        bulk(ret, b_recv, k)
+        rows = tiles_to_rows(ret[k].reshape(ROWS, 16, lanes), perm_ref[...], lanes)
+        block = jnp.concatenate([jnp.concatenate(r, axis=1) for r in rows], axis=0)
+        dims = (((0,), (0,)), ((), ()))
+        acc[...] += lax.dot_general(
+            mix[k, 0], block, dims, preferred_element_type=jnp.float32
+        ) + lax.dot_general(mix[k, 1], block, dims, preferred_element_type=jnp.float32)
+
+    stages = ((arrive, 0), (forward, 1), (multiply, 2), (relay, 3), (finish, 4), (combine, 5))
+
+    def step(s, carry):
+        for stage, lag in stages:
+
+            @pl.when(jnp.logical_and(s >= lag, s < lag + CHUNKS))
+            def _(stage=stage, lag=lag):
+                stage(s - lag)
+
+        return carry
+
+    lax.fori_loop(0, CHUNKS + 5, step, 0)
+    out_ref[...] = acc[...].astype(jnp.bfloat16)
+
+    def drain(k, carry):
+        bulk(outb, a_send, k)
+        bulk(back, b_send, k)
+        for which in range(4):
+            g_copy(k, which).wait_send()
+        for which in range(6):
+            q_copy(k, which).wait_send()
+        return carry
+
+    lax.fori_loop(0, CHUNKS, drain, 0)
 
 
 def routed_experts(
     moe_tokens, moe_gain, routes, route_weights, expert_gate, expert_up, expert_down
 ):
-    tok_rows, width = moe_tokens.shape
-    top_count = routes.shape[1]
-    experts = lax.axis_size("ep")
-    capacity = tok_rows * top_count * 5 // (4 * experts)
-    normed = rms_scale(moe_tokens.astype(jnp.float32), moe_gain).astype(jnp.bfloat16)
-    gate_weight = expert_gate[0]
-    up_weight = expert_up[0]
-    down_weight = expert_down[0]
-    slot_place = slot_places(routes[None], experts)
-    select_rows = dispatch_matrix(slot_place, capacity * experts)[0]
-    outgoing = jnp.dot(select_rows, normed, preferred_element_type=jnp.float32)
-    outgoing = outgoing.astype(jnp.bfloat16).reshape(capacity, experts, width)
-    slot_rows = lax.all_gather(
-        lax.all_to_all(outgoing, "ep", split_axis=1, concat_axis=1, tiled=True),
-        "tp",
-        axis=0,
-        tiled=True,
-    )
-    gate_value = jnp.dot(slot_rows, gate_weight, preferred_element_type=jnp.float32)
-    up_value = jnp.dot(slot_rows, up_weight, preferred_element_type=jnp.float32)
-    hidden = (jax.nn.silu(gate_value) * up_value).astype(jnp.bfloat16)
-    summed = lax.psum_scatter(
-        jnp.dot(hidden, down_weight, preferred_element_type=jnp.float32).astype(jnp.bfloat16),
-        "tp",
-        scatter_dimension=0,
-        tiled=True,
-    )
-    returned = lax.all_to_all(summed, "ep", split_axis=1, concat_axis=1, tiled=True)
-    flat_returned = returned.reshape(capacity * experts, width)
-    picked = flat_returned[slot_place[0]]
-    combined = jnp.sum(route_weights[:, :, None] * picked.astype(jnp.float32), axis=1)
-    return combined.astype(jnp.bfloat16)
+    tok, width = moe_tokens.shape
+    n_tp = lax.axis_size("tp")
+    hidden = expert_gate.shape[2]
+    lanes = width // 16
+    bf16 = jnp.bfloat16
+    vmem = pl.BlockSpec(memory_space=pltpu.VMEM)
+    hbm = pl.BlockSpec(memory_space=pl.ANY)
+    tiles = (CHUNKS, HALVES * N_YC, CAP, 16, lanes)
+    return pl.pallas_call(
+        functools.partial(experts_kernel, n_tp),
+        out_shape=jax.ShapeDtypeStruct((tok, width), bf16),
+        in_specs=[vmem, vmem, vmem, vmem, hbm, hbm, hbm],
+        out_specs=vmem,
+        scratch_shapes=[
+            pltpu.VMEM(tiles, bf16),
+            pltpu.VMEM(tiles, bf16),
+            pltpu.VMEM((CHUNKS, n_tp, ROWS, width), bf16),
+            pltpu.VMEM((CHUNKS, n_tp, ROWS, width), bf16),
+            pltpu.VMEM((CHUNKS, 2, ROWS, width // 2), bf16),
+            pltpu.VMEM((CHUNKS, 2, ROWS, width), bf16),
+            pltpu.VMEM(tiles, bf16),
+            pltpu.VMEM(tiles, bf16),
+            pltpu.VMEM((hidden // 128, width, 256), bf16),
+            pltpu.VMEM((width // 256, hidden, 256), bf16),
+            pltpu.VMEM((n_tp * ROWS, hidden), bf16),
+            pltpu.VMEM((tok, width), jnp.float32),
+            pltpu.VMEM((CHUNKS, 2, ROWS, tok), bf16),
+            pltpu.VMEM((256, 256), bf16),
+            pltpu.VMEM((tok, width), bf16),
+            pltpu.SemaphoreType.DMA((2,)),
+            pltpu.SemaphoreType.DMA((CHUNKS,)),
+            pltpu.SemaphoreType.DMA((CHUNKS,)),
+            pltpu.SemaphoreType.DMA((CHUNKS, 4)),
+            pltpu.SemaphoreType.DMA((CHUNKS, 4)),
+            pltpu.SemaphoreType.DMA((CHUNKS, 6)),
+            pltpu.SemaphoreType.DMA((CHUNKS, 6)),
+            pltpu.SemaphoreType.DMA((CHUNKS,)),
+            pltpu.SemaphoreType.DMA((CHUNKS,)),
+        ],
+        compiler_params=pltpu.CompilerParams(
+            collective_id=0, has_side_effects=True, vmem_limit_bytes=56 * 1024 * 1024
+        ),
+        cost_estimate=pl.CostEstimate(
+            flops=2 * 3 * CHUNKS * n_tp * ROWS * width * hidden,
+            bytes_accessed=3 * width * hidden * 2,
+            transcendentals=0,
+        ),
+    )(
+        moe_tokens,
+        moe_gain[None, :],
+        routes.T,
+        route_weights.T,
+        expert_gate,
+        expert_up,
+        expert_down,
+    )
 
 
 def shards(

time: 304 us -> 168 us (0.55)
  the two profiles are of different devices: /device:TPU:1 before, /device:TPU:25 now
where the time goes in v1:
time: 168 us; the launch traced here: 167 us
  Pallas kernels  137 us (82%)
  between operations  14.2 us (8%)
  starting transfers between devices  5.7 us (3%)
  local copies, waits for them, and re-layouts  3.41 us (2%)
  other arithmetic  3.41 us (2%)
  matrix products  3.07 us (2%)
    pallas_call x1, Pallas kernels, routed_experts(): pl.pallas_call(functools.partial(experts_kernel, n_tp), out_shape=jax.Sha...  137 us
    ppermute x2, starting transfers between devices, shifted(): return lax.ppermute(shard, axis, pairs)  5.66 us
  transfers between devices with their start and end apart: 3, of which 0 were waited for; matrix products, arithmetic and copies ran while one was open for 2% of the time, Pallas kernels for 82%

profile of v1, /device:TPU:25, one launch (start us, length us, event | category | flops | bytes accessed | tf_op | source)
XLA Modules:
  0.0 167.2 jit_solution(3911512278980047982)
XLA Ops:
  7.2 0.0 copy-start
  7.2 0.0 copy-start.3
  7.2 0.0 reduce-scatter.2.cloned.1.call-start
  7.2 0.8 slice.7
  8.0 3.8 %collective-permute-start.1 = (bf16[128,64]{0,1:T(8,128)(2,1)S(1)}, bf16[128,64]{0,1:T(8,128)(2,1)S(1)}, u32[]{:S(2)}, u32[]{:S(2)}) collective-permute-start(bf16[128,64]{0,1:T(8,128)(2,1)S(1)} %slice.7), channel_id=1, source_target_pairs={{0,4},{4,8},{8,12},{12,16},{16,20},{20,24},{24,28},{28,32},{32,36}... | collective-permute-start | bytes 49160 | tf_op jit(solution)/shard_map/ppermute | solution.py:32
  11.8 0.7 slice.6
  12.5 1.9 %collective-permute-start = (bf16[128,64]{0,1:T(8,128)(2,1)S(1)}, bf16[128,64]{0,1:T(8,128)(2,1)S(1)}, u32[]{:S(2)}, u32[]{:S(2)}) collective-permute-start(bf16[128,64]{0,1:T(8,128)(2,1)S(1)} %slice.6), channel_id=1, source_target_pairs={{0,4},{4,8},{8,12},{12,16},{16,20},{20,24},{24,28},{28,32},{32,36}... | collective-permute-start | bytes 49160 | tf_op jit(solution)/shard_map/ppermute | solution.py:32
  14.5 0.2 fusion.8
  14.6 0.0 collective-permute-done.1
  14.7 0.0 copy-start.2
  14.7 1.3 fusion.15
  16.0 0.0 copy-done.3
  16.0 0.1 broadcast_maximum_fusion
  16.0 0.2 fusion.2
  16.2 0.1 exponential_add_fusion
  16.3 0.0 collective-permute-done
  16.3 0.0 copy-done.2
  16.3 0.3 convolution_convert_fusion.1
  16.6 0.0 copy-done
  16.7 1.5 convolution_convert_fusion
  18.1 0.0 reduce-scatter.2.cloned.1.call-update
  18.1 0.0 copy-start.1
  18.1 137.3 %shard_map.140 = bf16[128,2048]{1,0:T(8,128)(2,1)} custom-call(bf16[128,2048]{1,0:T(8,128)(2,1)} %tokens_ref.1, f32[1,2048]{1,0:T(1,128)} %bitcast.31, s32[2,128]{1,0:T(2,128)} %bitcast.32, f32[2,128]{1,0:T(2,128)} %bitcast.33, bf16[1,2048,896]{2,1,0:T(8,128)(2,1)} %gate_ref.1, bf16[1,2048,896]{2,1,0:T(8,128)(2,1)} %up_ref.1, bf16[1,896,2048]{2,1,0:T(8,128)(2,1)} %down_ref.1), custom_call_target="tpu_custom_call" | custom-call | flops 14092861440 | bytes 11010048 | tf_op jit(solution)/shard_map/pallas_call | solution.py:454
  155.5 0.0 reduce-scatter.2.cloned.1.call-done
  155.5 1.1 fusion.4
  156.6 0.0 copy-done.1
  156.6 1.8 %fusion.6 = bf16[64,2048]{1,0:T(8,128)(2,1)} fusion(bf16[64,2048]{1,0:T(8,128)(2,1)} %reduce-scatter.2.cloned.1.call-done, f32[2048]{0:T(1024)S(1)} %copy-done.1, f32[64]{0:T(128)S(1)} %add_rsqrt_fusion), kind=kLoop, calls=%fused_computation.15 | loop fusion | flops 524288 | bytes 532736 | tf_op jit(solution)/shard_map/convert_element_type | solution.py:75
  158.4 1.9 %copy.18 = bf16[128,2048]{1,0:T(8,128)(2,1)} copy(bf16[128,2048]{1,0:T(8,128)(2,1)} %shard_map.140) | data formatting | bytes 1048576
  (4 shorter events, 0.0 us)
Async XLA Ops:
  7.2 9.5 %copy-start = (bf16[192,2048]{1,0:T(8,128)(2,1)S(1)}, bf16[192,2048]{1,0:T(8,128)(2,1)}, u32[]{:S(2)}) copy-start(bf16[192,2048]{1,0:T(8,128)(2,1)} %param.17) | copy-start | bytes 2359300
  7.2 8.8 %copy-start.3 = (f32[3]{0:T(128)S(1)}, f32[3]{0:T(128)}, u32[]{:S(2)}) copy-start(f32[3]{0:T(128)} %param.16) | copy-start | bytes 40
  7.2 148.3 %reduce-scatter.2.cloned.1.call-start = ((), (), s32[]{:S(2)}) async-start(), calls=%async_computation.1 | async-start | bytes 1310720 | tf_op jit(solution)/shard_map/reduce_scatter | solution.py:69
  8.0 6.6 %collective-permute-start.1 = (bf16[128,64]{0,1:T(8,128)(2,1)S(1)}, bf16[128,64]{0,1:T(8,128)(2,1)S(1)}, u32[]{:S(2)}, u32[]{:S(2)}) collective-permute-start(bf16[128,64]{0,1:T(8,128)(2,1)S(1)} %slice.7), channel_id=1, source_target_pairs={{0,4},{4,8},{8,12},{12,16},{16,20},{20,24},{24,28},{28,32},{32,36}... | collective-permute-start | bytes 49160 | tf_op jit(solution)/shard_map/ppermute | solution.py:32
  12.5 3.8 %collective-permute-start = (bf16[128,64]{0,1:T(8,128)(2,1)S(1)}, bf16[128,64]{0,1:T(8,128)(2,1)S(1)}, u32[]{:S(2)}, u32[]{:S(2)}) collective-permute-start(bf16[128,64]{0,1:T(8,128)(2,1)S(1)} %slice.6), channel_id=1, source_target_pairs={{0,4},{4,8},{8,12},{12,16},{16,20},{20,24},{24,28},{28,32},{32,36}... | collective-permute-start | bytes 49160 | tf_op jit(solution)/shard_map/ppermute | solution.py:32
  14.7 1.7 copy-start.2
  18.1 138.5 %copy-start.1 = (f32[2048]{0:T(1024)S(1)}, f32[2048]{0:T(1024)}, u32[]{:S(2)}) copy-start(f32[2048]{0:T(1024)} %param.18) | copy-start | bytes 24580
Sparse Core Ops, SparseCore 0:
  18.3 28.9 reduce-scatter.1

commit v2 on v1

--- a/solution.py
+++ b/solution.py
@@ -19,60 +19,10 @@
 CAP = 5
 CHUNKS = 4
 HALVES = 2
-OFFSETS = ((0, 1), (2, 6), (3, 5), (4, 7))
-SELF_CHUNK = 0
+OFFSETS = ((2, 6), (4, 7), (3, 5), (0, 1))
+SELF_CHUNK = 3
 ROWS = HALVES * N_YC * CAP
 GROUPS = ROWS // 16
-GROUP_ROWS = N_YC * CAP
-
-
-def shifted(shard, axis, by):
-    size = lax.axis_size(axis)
-    pairs = [(i, i + by) for i in range(size) if 0 <= i + by < size]
-    return lax.ppermute(shard, axis, pairs)
-
-
-def rms_scale(rows_in, gain):
-    squares = jnp.mean(rows_in * rows_in, axis=-1, keepdims=True)
-    return rows_in * lax.rsqrt(squares + norm_eps) * gain
-
-
-def mixer(queries, key_rows, value_rows, sink_logits, out_weight, mix_gain):
-    tok_rows = queries.shape[0]
-    kv_local = key_rows.shape[1] // HDIM
-    group_size = queries.shape[1] // key_rows.shape[1]
-    rim_rows = (key_rows[tok_rows - WINDOW :], value_rows[tok_rows - WINDOW :])
-    prev_keys, prev_values = shifted((rim_rows[0], rim_rows[1]), "ep", 1)
-    all_keys = jnp.concatenate([prev_keys, key_rows], axis=0).reshape(
-        tok_rows + WINDOW, kv_local, HDIM
-    )
-    all_values = jnp.concatenate([prev_values, value_rows], axis=0).reshape(
-        tok_rows + WINDOW, kv_local, HDIM
-    )
-    offset = lax.axis_index("ep") * tok_rows
-    query_pos = offset + jnp.arange(tok_rows, dtype=jnp.int32)
-    key_pos = offset - WINDOW + jnp.arange(tok_rows + WINDOW, dtype=jnp.int32)
-    distance = query_pos[:, None] - key_pos[None, :]
-    allowed = (distance >= 0) & (distance < WINDOW) & (key_pos >= 0)[None, :]
-    grouped = queries.reshape(tok_rows, kv_local, group_size, HDIM)
-    scores = jnp.einsum(
-        "qkgd,jkd->kgqj", grouped, all_keys, preferred_element_type=jnp.float32
-    ) * HDIM ** (-0.5)
-    logits = jnp.where(allowed, scores, masked_value)
-    sink_logit = sink_logits.reshape(kv_local, group_size)[:, :, None, None]
-    top_value = jnp.maximum(jnp.max(logits, axis=-1, keepdims=True), sink_logit)
-    exponent = jnp.exp(logits - top_value)
-    denominator = jnp.sum(exponent, axis=-1, keepdims=True) + jnp.exp(sink_logit - top_value)
-    probs = (exponent / denominator).astype(jnp.bfloat16)
-    attended = jnp.einsum("kgqj,jkd->qkgd", probs, all_values, preferred_element_type=jnp.float32)
-    attended = attended.astype(jnp.bfloat16).reshape(tok_rows, -1)
-    projected = lax.psum_scatter(
-        jnp.dot(attended, out_weight, preferred_element_type=jnp.float32).astype(jnp.bfloat16),
-        "tp",
-        scatter_dimension=0,
-        tiled=True,
-    ).astype(jnp.float32)
-    return rms_scale(projected, mix_gain).astype(jnp.bfloat16)
 
 
 def pick(index, table):
@@ -109,15 +59,22 @@
     ]
 
 
-def experts_kernel(
+def layer_kernel(
     n_tp,
     tokens_ref,
     gain_ref,
     routes_ref,
     weights_ref,
+    queries_ref,
+    keys_ref,
+    values_ref,
+    sink_ref,
+    mix_gain_ref,
     gate_ref,
     up_ref,
     down_ref,
+    project_ref,
+    mixed_ref,
     out_ref,
     outb,
     recv,
@@ -134,6 +91,16 @@
     mix,
     perm_ref,
     row_ref,
+    halo,
+    attended,
+    wproj,
+    mpart,
+    m1,
+    m2,
+    h_send,
+    h_recv,
+    m_send,
+    m_recv,
     w_sem,
     a_send,
     a_recv,
@@ -178,6 +145,8 @@
         pltpu.make_async_copy(
             down_ref.at[0, :, pl.ds(256 * n, 256)], wdn.at[n], w_sem.at[1]
         ).start()
+
+    pltpu.make_async_copy(project_ref, wproj, w_sem.at[2]).start()
 
     tok = tokens_ref.shape[0]
     e_rows = [routes_ref[0:1, :], routes_ref[1:2, :]]
@@ -278,19 +247,143 @@
         for g in range(GROUPS):
             flat[16 * g : 16 * g + 16] = tiles[g]
 
-        @pl.when(k == 0)
-        def _():
-            pl.semaphore_wait(barrier, N_Z * N_YC - 1 + 2)
-
-        @pl.when(k == SELF_CHUNK)
-        def _():
-            recv[k, yc] = outb[k, yc]
-
+        return carry
+
+    with jax.named_scope("dispatch"):
+        lax.fori_loop(0, CHUNKS, dispatch, 0)
+    with jax.named_scope("barrier_wait"):
+        pl.semaphore_wait(barrier, N_Z * N_YC - 1 + 2)
+    follower = lax.rem(me + 1, jnp.int32(N_Z * N_YC))
+
+    def h_copy(which):
+        ref = (keys_ref, values_ref)[which]
+        return pltpu.make_async_remote_copy(
+            src_ref=ref.at[:, pl.ds(ref.shape[1] - WINDOW, WINDOW)],
+            dst_ref=halo.at[which],
+            send_sem=h_send.at[which],
+            recv_sem=h_recv.at[which],
+            device_id={"ep": follower},
+            device_id_type=MESH,
+        )
+
+    h_copy(0).start()
+    h_copy(1).start()
+    recv[SELF_CHUNK, yc] = outb[SELF_CHUNK, yc]
+
+    def send(k, carry):
         spread(a_copy, k)
         return carry
 
-    lax.fori_loop(0, CHUNKS, dispatch, 0)
+    with jax.named_scope("send"):
+        lax.fori_loop(0, CHUNKS, send, 0)
     acc[...] = jnp.zeros_like(acc)
+
+    heads = queries_ref.shape[0] // HDIM
+    sinks = jnp.concatenate(
+        [jnp.full((1, WINDOW), sink_ref[h], jnp.float32) for h in range(heads)], axis=1
+    )
+    key_i = lax.broadcasted_iota(jnp.int32, (2 * WINDOW, heads * WINDOW), 0)
+    query_i = lax.broadcasted_iota(jnp.int32, (2 * WINDOW, heads * WINDOW), 1) & (WINDOW - 1)
+    in_window = jnp.logical_and(key_i > query_i, key_i <= query_i + WINDOW)
+
+    def attend(b, keys, values, allowed):
+        at = slice(WINDOW * b, WINDOW * b + WINDOW)
+        block = jnp.concatenate(
+            [queries_ref[HDIM * h : HDIM * h + HDIM, at] for h in range(heads)], axis=1
+        )
+        scores = lax.dot_general(
+            keys, block, (((0,), (0,)), ((), ())), preferred_element_type=jnp.float32
+        ) * HDIM ** (-0.5)
+        logits = jnp.where(allowed, scores, masked_value)
+        top = jnp.maximum(jnp.max(logits, axis=0, keepdims=True), sinks)
+        exponent = jnp.exp(logits - top)
+        denominator = jnp.sum(exponent, axis=0, keepdims=True) + jnp.exp(sinks - top)
+        probs = (exponent / denominator).astype(jnp.bfloat16)
+        result = jnp.dot(values, probs, preferred_element_type=jnp.float32).astype(jnp.bfloat16)
+        for h in range(heads):
+            attended[HDIM * h : HDIM * h + HDIM, at] = result[:, WINDOW * h : WINDOW * h + WINDOW]
+
+    blocks = queries_ref.shape[1] // WINDOW
+    with jax.named_scope("attend_own"):
+        for b in range(1, blocks):
+            at = slice(WINDOW * (b - 1), WINDOW * (b + 1))
+            attend(b, keys_ref[:, at], values_ref[:, at], in_window)
+    with jax.named_scope("halo_wait"):
+        h_copy(0).wait_recv()
+        h_copy(1).wait_recv()
+    with jax.named_scope("attend_halo"):
+        first = slice(0, WINDOW)
+        attend(
+            0,
+            jnp.concatenate([halo[0], keys_ref[:, first]], axis=1),
+            jnp.concatenate([halo[1], values_ref[:, first]], axis=1),
+            jnp.logical_and(in_window, jnp.logical_or(key_i >= WINDOW, me > 0)),
+        )
+    with jax.named_scope("project"):
+        pltpu.make_async_copy(wproj, wproj, w_sem.at[2]).wait()
+        own_rows = mpart.shape[1]
+        for n in range(width // 512):
+            at = slice(512 * n, 512 * n + 512)
+            part = lax.dot_general(
+                attended[...],
+                wproj[:, at],
+                (((0,), (0,)), ((), ())),
+                preferred_element_type=jnp.float32,
+            ).astype(jnp.bfloat16)
+            mpart[:, :, at] = part.reshape(n_tp, own_rows, 512)
+    across = lax.rem(tp + 2, jnp.int32(n_tp))
+    left_half = pl.ds(0, half)
+    right_half = pl.ds(half, half)
+
+    def m_copy(which):
+        if which == 0:
+            src, dst, to = mpart.at[across, :, left_half], m1.at[0], right
+        elif which == 1:
+            src, dst, to = mpart.at[across, :, right_half], m1.at[1], left
+        elif which == 2:
+            src, dst, to = mpart.at[right, :, right_half], m2.at[0, :, right_half], right
+        elif which == 3:
+            src, dst, to = mpart.at[left, :, left_half], m2.at[1, :, left_half], left
+        elif which == 4:
+            src, dst, to = mpart.at[right, :, left_half], m2.at[0, :, left_half], right
+        else:
+            src, dst, to = mpart.at[left, :, right_half], m2.at[1, :, right_half], left
+        return pltpu.make_async_remote_copy(
+            src_ref=src,
+            dst_ref=dst,
+            send_sem=m_send.at[which],
+            recv_sem=m_recv.at[which],
+            device_id={"tp": to},
+            device_id_type=MESH,
+        )
+
+    for which in range(4):
+        m_copy(which).start()
+
+    def mixer_relay():
+        m_copy(0).wait_recv()
+        mpart[right, :, left_half] = (
+            mpart[right, :, left_half].astype(jnp.float32) + m1[0].astype(jnp.float32)
+        ).astype(jnp.bfloat16)
+        m_copy(4).start()
+        m_copy(1).wait_recv()
+        mpart[left, :, right_half] = (
+            mpart[left, :, right_half].astype(jnp.float32) + m1[1].astype(jnp.float32)
+        ).astype(jnp.bfloat16)
+        m_copy(5).start()
+
+    def mixer_finish():
+        for which in range(2, 6):
+            m_copy(which).wait_recv()
+        total = (
+            mpart[tp].astype(jnp.float32)
+            + m2[0].astype(jnp.float32)
+            + m2[1].astype(jnp.float32)
+        )
+        squares = jnp.mean(total * total, axis=-1, keepdims=True)
+        mixed_ref[...] = (total * lax.rsqrt(squares + norm_eps) * mix_gain_ref[...]).astype(
+            jnp.bfloat16
+        )
 
     low = pl.ds(0, half)
     high = pl.ds(half, half)
@@ -336,7 +429,8 @@
         )
 
     def arrive(k):
-        bulk(recv, a_recv, k)
+        with jax.named_scope("arrive_wait"):
+            bulk(recv, a_recv, k)
         rows = tiles_to_rows(recv[k].reshape(ROWS, 16, lanes), perm_ref[...], lanes)
         for g in range(GROUPS):
             for s in range(16):
@@ -345,10 +439,11 @@
         g_copy(k, 1).start()
 
     def forward(k):
-        g_copy(k, 0).wait_recv()
-        g_copy(k, 2).start()
-        g_copy(k, 1).wait_recv()
-        g_copy(k, 3).start()
+        with jax.named_scope("forward_wait"):
+            g_copy(k, 0).wait_recv()
+            g_copy(k, 2).start()
+            g_copy(k, 1).wait_recv()
+            g_copy(k, 3).start()
 
     def multiply(k):
         @pl.when(k == 0)
@@ -356,8 +451,9 @@
             pltpu.make_async_copy(wgu, wgu, w_sem.at[0]).wait()
             pltpu.make_async_copy(wdn, wdn, w_sem.at[1]).wait()
 
-        g_copy(k, 2).wait_recv()
-        g_copy(k, 3).wait_recv()
+        with jax.named_scope("multiply_wait"):
+            g_copy(k, 2).wait_recv()
+            g_copy(k, 3).wait_recv()
         for n in range(gate_tiles):
             both = jnp.dot(
                 xbuf[k].reshape(n_tp * ROWS, width), wgu[n], preferred_element_type=jnp.float32
@@ -375,7 +471,8 @@
             q_copy(k, which).start()
 
     def relay(k):
-        q_copy(k, 0).wait_recv()
+        with jax.named_scope("relay_wait"):
+            q_copy(k, 0).wait_recv()
         pbuf[k, 2, :, low] = (
             pbuf[k, 2, :, low].astype(jnp.float32) + r1[k, 0].astype(jnp.float32)
         ).astype(jnp.bfloat16)
@@ -387,8 +484,9 @@
         q_copy(k, 5).start()
 
     def finish(k):
-        for which in range(2, 6):
-            q_copy(k, which).wait_recv()
+        with jax.named_scope("finish_wait"):
+            for which in range(2, 6):
+                q_copy(k, which).wait_recv()
         total = (
             pbuf[k, 0].astype(jnp.float32)
             + r2[k, 0].astype(jnp.float32)
@@ -406,7 +504,8 @@
         spread(b_copy, k)
 
     def combine(k):
-        bulk(ret, b_recv, k)
+        with jax.named_scope("combine_wait"):
+            bulk(ret, b_recv, k)
         rows = tiles_to_rows(ret[k].reshape(ROWS, 16, lanes), perm_ref[...], lanes)
         block = jnp.concatenate([jnp.concatenate(r, axis=1) for r in rows], axis=0)
         dims = (((0,), (0,)), ((), ()))
@@ -418,10 +517,22 @@
 
     def step(s, carry):
         for stage, lag in stages:
+            if stage is forward:
+
+                @pl.when(s == 0)
+                def _():
+                    with jax.named_scope("mixer_relay"):
+                        mixer_relay()
+
+                @pl.when(s == 3)
+                def _():
+                    with jax.named_scope("mixer_finish"):
+                        mixer_finish()
 
             @pl.when(jnp.logical_and(s >= lag, s < lag + CHUNKS))
             def _(stage=stage, lag=lag):
-                stage(s - lag)
+                with jax.named_scope(stage.__name__):
+                    stage(s - lag)
 
         return carry
 
@@ -437,25 +548,48 @@
             q_copy(k, which).wait_send()
         return carry
 
-    lax.fori_loop(0, CHUNKS, drain, 0)
-
-
-def routed_experts(
-    moe_tokens, moe_gain, routes, route_weights, expert_gate, expert_up, expert_down
+    with jax.named_scope("drain"):
+        for which in range(2):
+            h_copy(which).wait_send()
+        for which in range(6):
+            m_copy(which).wait_send()
+        lax.fori_loop(0, CHUNKS, drain, 0)
+
+
+def shards(
+    queries,
+    key_rows,
+    value_rows,
+    sink_logits,
+    out_weight,
+    mix_gain,
+    moe_tokens,
+    moe_gain,
+    routes,
+    route_weights,
+    expert_gate,
+    expert_up,
+    expert_down,
 ):
     tok, width = moe_tokens.shape
     n_tp = lax.axis_size("tp")
     hidden = expert_gate.shape[2]
     lanes = width // 16
+    own_rows = queries.shape[0] // n_tp
     bf16 = jnp.bfloat16
     vmem = pl.BlockSpec(memory_space=pltpu.VMEM)
+    smem = pl.BlockSpec(memory_space=pltpu.SMEM)
     hbm = pl.BlockSpec(memory_space=pl.ANY)
+    dma = pltpu.SemaphoreType.DMA
     tiles = (CHUNKS, HALVES * N_YC, CAP, 16, lanes)
     return pl.pallas_call(
-        functools.partial(experts_kernel, n_tp),
-        out_shape=jax.ShapeDtypeStruct((tok, width), bf16),
-        in_specs=[vmem, vmem, vmem, vmem, hbm, hbm, hbm],
-        out_specs=vmem,
+        functools.partial(layer_kernel, n_tp),
+        out_shape=(
+            jax.ShapeDtypeStruct((own_rows, width), bf16),
+            jax.ShapeDtypeStruct((tok, width), bf16),
+        ),
+        in_specs=[vmem] * 7 + [smem, vmem] + [hbm] * 4,
+        out_specs=(vmem, vmem),
         scratch_shapes=[
             pltpu.VMEM(tiles, bf16),
             pltpu.VMEM(tiles, bf16),
@@ -472,55 +606,44 @@
             pltpu.VMEM((CHUNKS, 2, ROWS, tok), bf16),
             pltpu.VMEM((256, 256), bf16),
             pltpu.VMEM((tok, width), bf16),
-            pltpu.SemaphoreType.DMA((2,)),
-            pltpu.SemaphoreType.DMA((CHUNKS,)),
-            pltpu.SemaphoreType.DMA((CHUNKS,)),
-            pltpu.SemaphoreType.DMA((CHUNKS, 4)),
-            pltpu.SemaphoreType.DMA((CHUNKS, 4)),
-            pltpu.SemaphoreType.DMA((CHUNKS, 6)),
-            pltpu.SemaphoreType.DMA((CHUNKS, 6)),
-            pltpu.SemaphoreType.DMA((CHUNKS,)),
-            pltpu.SemaphoreType.DMA((CHUNKS,)),
+            pltpu.VMEM((2, HDIM, WINDOW), bf16),
+            pltpu.VMEM((queries.shape[1], queries.shape[0]), bf16),
+            pltpu.VMEM(out_weight.shape, bf16),
+            pltpu.VMEM((n_tp, own_rows, width), bf16),
+            pltpu.VMEM((2, own_rows, width // 2), bf16),
+            pltpu.VMEM((2, own_rows, width), bf16),
+            dma((2,)),
+            dma((2,)),
+            dma((6,)),
+            dma((6,)),
+            dma((3,)),
+            dma((CHUNKS,)),
+            dma((CHUNKS,)),
+            dma((CHUNKS, 4)),
+            dma((CHUNKS, 4)),
+            dma((CHUNKS, 6)),
+            dma((CHUNKS, 6)),
+            dma((CHUNKS,)),
+            dma((CHUNKS,)),
         ],
         compiler_params=pltpu.CompilerParams(
-            collective_id=0, has_side_effects=True, vmem_limit_bytes=56 * 1024 * 1024
-        ),
-        cost_estimate=pl.CostEstimate(
-            flops=2 * 3 * CHUNKS * n_tp * ROWS * width * hidden,
-            bytes_accessed=3 * width * hidden * 2,
-            transcendentals=0,
+            collective_id=0, has_side_effects=True, vmem_limit_bytes=58 * 1024 * 1024
         ),
     )(
         moe_tokens,
         moe_gain[None, :],
         routes.T,
         route_weights.T,
+        queries.T,
+        key_rows.T,
+        value_rows.T,
+        sink_logits,
+        mix_gain[None, :],
         expert_gate,
         expert_up,
         expert_down,
+        out_weight,
     )
-
-
-def shards(
-    queries,
-    key_rows,
-    value_rows,
-    sink_logits,
-    out_weight,
-    mix_gain,
-    moe_tokens,
-    moe_gain,
-    routes,
-    route_weights,
-    expert_gate,
-    expert_up,
-    expert_down,
-):
-    mixed = mixer(queries, key_rows, value_rows, sink_logits, out_weight, mix_gain)
-    moe_out = routed_experts(
-        moe_tokens, moe_gain, routes, route_weights, expert_gate, expert_up, expert_down
-    )
-    return (mixed, moe_out)
 
 
 def solution(mesh):

time: 168 us -> 136 us (0.81)
  the two profiles are of different devices: /device:TPU:25 before, /device:TPU:1 now
where the time goes in v2:
time: 136 us
  Pallas kernels  132 us (97%)
  local copies, waits for them, and re-layouts  3.55 us (3%)
    pallas_call x1, Pallas kernels, shards(): pl.pallas_call(functools.partial(layer_kernel, n_tp), out_shape=(jax.Shap...  132 us
    unnamed x2, local copies, waits for them, and re-layouts  3.55 us

profile of v2, /device:TPU:1, one launch (start us, length us, event | category | flops | bytes accessed | tf_op | source)
XLA Modules:
  0.0 136.2 jit_solution(5975041124034138981)
XLA Ops:
  0.6 132.0 %shard_map.140 = (bf16[64,2048]{1,0:T(8,128)(2,1)}, bf16[128,2048]{1,0:T(8,128)(2,1)}) custom-call(bf16[128,2048]{1,0:T(8,128)(2,1)} %tokens_ref.1, f32[1,2048]{1,0:T(1,128)} %bitcast.10, s32[2,128]{1,0:T(2,128)} %bitcast.12, f32[2,128]{1,0:T(2,128)} %bitcast.13, bf16[192,256]{1,0:T(8,128)(2,1)} %bitcast.7, bf16[64,256]{1,0:T(8,128)(2,1)} %bitcast.8, ...), custom_call_target="tpu_custom_call" | custom-call | tf_op jit(solution)/shard_map/pallas_call | solution.py:585
  132.6 1.7 %copy.17 = bf16[64,2048]{1,0:T(8,128)(2,1)} copy(bf16[64,2048]{1,0:T(8,128)(2,1)} %get-tuple-element.4) | data formatting | bytes 524288
  134.3 1.9 %copy.18 = bf16[128,2048]{1,0:T(8,128)(2,1)} copy(bf16[128,2048]{1,0:T(8,128)(2,1)} %get-tuple-element.5) | data formatting | bytes 1048576

commit v3 on v2

--- a/solution.py
+++ b/solution.py
@@ -20,16 +20,14 @@
 CHUNKS = 4
 HALVES = 2
 OFFSETS = ((2, 6), (4, 7), (3, 5), (0, 1))
+SETTLE_ROWS = 64
 SELF_CHUNK = 3
+ORDER = (
+    "D3 B S3 D0 S0 O D1 D2 H Q S1 A3 A0 S2 F3 A1 F0 M3 F1 A2 M0 W1 F2 L1 T0 M2 E1 L0 T2 E0 L2 T3 "
+    "C1 E2 L3 P C0 E3 R C2 X C3"
+)
 ROWS = HALVES * N_YC * CAP
 GROUPS = ROWS // 16
-
-
-def pick(index, table):
-    value = jnp.int32(table[-1])
-    for place in range(len(table) - 2, -1, -1):
-        value = jnp.where(index == place, jnp.int32(table[place]), value)
-    return value
 
 
 def rows_to_tiles(block, perm, width):
@@ -61,6 +59,21 @@
 
 def layer_kernel(
     n_tp,
+    tokens_in,
+    gain_in,
+    routes_in,
+    weights_in,
+    queries_in,
+    keys_in,
+    values_in,
+    sink_in,
+    mix_gain_in,
+    gate_ref,
+    up_ref,
+    down_ref,
+    project_ref,
+    mixed_out,
+    moe_out,
     tokens_ref,
     gain_ref,
     routes_ref,
@@ -70,10 +83,6 @@
     values_ref,
     sink_ref,
     mix_gain_ref,
-    gate_ref,
-    up_ref,
-    down_ref,
-    project_ref,
     mixed_ref,
     out_ref,
     outb,
@@ -97,6 +106,8 @@
     mpart,
     m1,
     m2,
+    i_sem,
+    o_sem,
     h_send,
     h_recv,
     m_send,
@@ -123,16 +134,34 @@
     right = lax.rem(tp + 1, jnp.int32(n_tp))
     left = lax.rem(tp + n_tp - 1, jnp.int32(n_tp))
 
+    inputs = (
+        (routes_in, routes_ref),
+        (tokens_in, tokens_ref),
+        (gain_in, gain_ref),
+        (weights_in, weights_ref),
+        (keys_in, keys_ref),
+        (values_in, values_ref),
+        (queries_in, queries_ref),
+        (sink_in, sink_ref),
+        (mix_gain_in, mix_gain_ref),
+    )
+    for n, (src, dst) in enumerate(inputs):
+        pltpu.make_async_copy(src, dst, i_sem.at[n]).start()
+
     barrier = pltpu.get_barrier_semaphore()
 
+    n_ep = N_Z * N_YC
+
     def greet(i, carry):
-        @pl.when(i != me)
+        other = lax.rem(me + n_ep // 2 + i, jnp.int32(n_ep))
+
+        @pl.when(other != me)
         def _():
-            pl.semaphore_signal(barrier, inc=1, device_id={"ep": i}, device_id_type=MESH)
+            pl.semaphore_signal(barrier, inc=1, device_id={"ep": other}, device_id_type=MESH)
 
         return carry
 
-    lax.fori_loop(0, N_Z * N_YC, greet, 0)
+    lax.fori_loop(0, n_ep, greet, 0)
     pl.semaphore_signal(barrier, inc=1, device_id={"tp": right}, device_id_type=MESH)
     pl.semaphore_signal(barrier, inc=1, device_id={"tp": left}, device_id_type=MESH)
 
@@ -147,6 +176,9 @@
         ).start()
 
     pltpu.make_async_copy(project_ref, wproj, w_sem.at[2]).start()
+
+    for n, (src, dst) in enumerate(inputs):
+        pltpu.make_async_copy(src, dst, i_sem.at[n]).wait()
 
     tok = tokens_ref.shape[0]
     e_rows = [routes_ref[0:1, :], routes_ref[1:2, :]]
@@ -183,8 +215,7 @@
     row_ref[...] = (x * lax.rsqrt(squares + norm_eps) * gain_ref[...]).astype(jnp.bfloat16)
 
     def peer(i, y, sign, k):
-        distance = pick(k, [pair[i] for pair in OFFSETS])
-        return lax.rem(z + sign * distance + N_Z, jnp.int32(N_Z)) * N_YC + y
+        return lax.rem(z + (sign * OFFSETS[k][i]) % N_Z, jnp.int32(N_Z)) * N_YC + y
 
     def a_copy(k, i, y):
         return pltpu.make_async_remote_copy(
@@ -207,13 +238,14 @@
         )
 
     def spread(copy_of, k):
-        def one(y, carry):
+        def one(j, carry):
+            y = (yc + 1 + j) & (N_YC - 1)
             for i in range(HALVES):
-                if i == 0:
-
-                    @pl.when(jnp.logical_not(jnp.logical_and(k == SELF_CHUNK, y == yc)))
+                if OFFSETS[k][i] == 0:
+
+                    @pl.when(y != yc)
                     def _():
-                        copy_of(k, 0, y).start()
+                        copy_of(k, i, y).start()
                 else:
                     copy_of(k, i, y).start()
             return carry
@@ -221,17 +253,11 @@
         lax.fori_loop(0, N_YC, one, 0)
 
     def bulk(buffer, sem, k):
-        @pl.when(k == SELF_CHUNK)
-        def _():
-            view = buffer.at[k, pl.ds(0, HALVES * N_YC - 1)]
-            pltpu.make_async_copy(view, view, sem.at[k]).wait()
-
-        @pl.when(k != SELF_CHUNK)
-        def _():
-            view = buffer.at[k]
-            pltpu.make_async_copy(view, view, sem.at[k]).wait()
-
-    def dispatch(k, carry):
+        count = HALVES * N_YC - (k == SELF_CHUNK)
+        view = buffer.at[k, pl.ds(0, count)]
+        pltpu.make_async_copy(view, view, sem.at[k]).wait()
+
+    def dispatch(k):
         row_id = lax.broadcasted_iota(jnp.int32, (ROWS, tok), 0) + k * ROWS
         hits = [row_id == s for s in slots]
         select = jnp.where(jnp.logical_or(hits[0], hits[1]), 1.0, 0.0).astype(jnp.bfloat16)
@@ -246,13 +272,9 @@
         flat = outb.at[k].reshape(ROWS, 16, lanes)
         for g in range(GROUPS):
             flat[16 * g : 16 * g + 16] = tiles[g]
-
-        return carry
-
-    with jax.named_scope("dispatch"):
-        lax.fori_loop(0, CHUNKS, dispatch, 0)
-    with jax.named_scope("barrier_wait"):
-        pl.semaphore_wait(barrier, N_Z * N_YC - 1 + 2)
+        if k == SELF_CHUNK:
+            recv[k, yc] = outb[k, yc]
+
     follower = lax.rem(me + 1, jnp.int32(N_Z * N_YC))
 
     def h_copy(which):
@@ -266,21 +288,17 @@
             device_id_type=MESH,
         )
 
-    h_copy(0).start()
-    h_copy(1).start()
-    recv[SELF_CHUNK, yc] = outb[SELF_CHUNK, yc]
-
-    def send(k, carry):
+    def begin():
+        pl.semaphore_wait(barrier, n_ep - 1 + 2)
+        h_copy(0).start()
+        h_copy(1).start()
+
+    def send(k):
         spread(a_copy, k)
-        return carry
-
-    with jax.named_scope("send"):
-        lax.fori_loop(0, CHUNKS, send, 0)
-    acc[...] = jnp.zeros_like(acc)
 
     heads = queries_ref.shape[0] // HDIM
     sinks = jnp.concatenate(
-        [jnp.full((1, WINDOW), sink_ref[h], jnp.float32) for h in range(heads)], axis=1
+        [jnp.broadcast_to(sink_ref[0:1, h : h + 1], (1, WINDOW)) for h in range(heads)], axis=1
     )
     key_i = lax.broadcasted_iota(jnp.int32, (2 * WINDOW, heads * WINDOW), 0)
     query_i = lax.broadcasted_iota(jnp.int32, (2 * WINDOW, heads * WINDOW), 1) & (WINDOW - 1)
@@ -304,14 +322,35 @@
             attended[HDIM * h : HDIM * h + HDIM, at] = result[:, WINDOW * h : WINDOW * h + WINDOW]
 
     blocks = queries_ref.shape[1] // WINDOW
-    with jax.named_scope("attend_own"):
+    own_rows = mpart.shape[1]
+    block_parts = WINDOW // own_rows
+
+    def project(b):
+        at_rows = slice(WINDOW * b, WINDOW * b + WINDOW)
+        for n in range(width // 512):
+            at = slice(512 * n, 512 * n + 512)
+            part = lax.dot_general(
+                attended[:, at_rows],
+                wproj[:, at],
+                (((0,), (0,)), ((), ())),
+                preferred_element_type=jnp.float32,
+            ).astype(jnp.bfloat16)
+            mpart[block_parts * b : block_parts * b + block_parts, :, at] = part.reshape(
+                block_parts, own_rows, 512
+            )
+
+    def mixer_own():
         for b in range(1, blocks):
             at = slice(WINDOW * (b - 1), WINDOW * (b + 1))
             attend(b, keys_ref[:, at], values_ref[:, at], in_window)
-    with jax.named_scope("halo_wait"):
-        h_copy(0).wait_recv()
-        h_copy(1).wait_recv()
-    with jax.named_scope("attend_halo"):
+        pltpu.make_async_copy(wproj, wproj, w_sem.at[2]).wait()
+        for b in range(1, blocks):
+            project(b)
+
+    def mixer_halo():
+        with jax.named_scope("halo_wait"):
+            h_copy(0).wait_recv()
+            h_copy(1).wait_recv()
         first = slice(0, WINDOW)
         attend(
             0,
@@ -319,18 +358,8 @@
             jnp.concatenate([halo[1], values_ref[:, first]], axis=1),
             jnp.logical_and(in_window, jnp.logical_or(key_i >= WINDOW, me > 0)),
         )
-    with jax.named_scope("project"):
-        pltpu.make_async_copy(wproj, wproj, w_sem.at[2]).wait()
-        own_rows = mpart.shape[1]
-        for n in range(width // 512):
-            at = slice(512 * n, 512 * n + 512)
-            part = lax.dot_general(
-                attended[...],
-                wproj[:, at],
-                (((0,), (0,)), ((), ())),
-                preferred_element_type=jnp.float32,
-            ).astype(jnp.bfloat16)
-            mpart[:, :, at] = part.reshape(n_tp, own_rows, 512)
+        project(0)
+
     across = lax.rem(tp + 2, jnp.int32(n_tp))
     left_half = pl.ds(0, half)
     right_half = pl.ds(half, half)
@@ -357,8 +386,13 @@
             device_id_type=MESH,
         )
 
-    for which in range(4):
-        m_copy(which).start()
+    def mixer_transit():
+        m_copy(0).start()
+        m_copy(1).start()
+
+    def mixer_direct():
+        m_copy(2).start()
+        m_copy(3).start()
 
     def mixer_relay():
         m_copy(0).wait_recv()
@@ -384,6 +418,7 @@
         mixed_ref[...] = (total * lax.rsqrt(squares + norm_eps) * mix_gain_ref[...]).astype(
             jnp.bfloat16
         )
+        pltpu.make_async_copy(mixed_ref, mixed_out, o_sem.at[0]).start()
 
     low = pl.ds(0, half)
     high = pl.ds(half, half)
@@ -445,9 +480,8 @@
             g_copy(k, 1).wait_recv()
             g_copy(k, 3).start()
 
-    def multiply(k):
-        @pl.when(k == 0)
-        def _():
+    def multiply(k, sends=True):
+        if k == first_multiplied:
             pltpu.make_async_copy(wgu, wgu, w_sem.at[0]).wait()
             pltpu.make_async_copy(wdn, wdn, w_sem.at[1]).wait()
 
@@ -467,6 +501,13 @@
             pbuf[k, :, :, 256 * n : 256 * n + 256] = part.astype(jnp.bfloat16).reshape(
                 n_tp, ROWS, 256
             )
+            if sends and n == down_tiles // 2 - 1:
+                q_copy(k, 0).start()
+        if sends:
+            for which in range(1, 4):
+                q_copy(k, which).start()
+
+    def hand_on(k):
         for which in range(4):
             q_copy(k, which).start()
 
@@ -496,9 +537,7 @@
         flat = back.at[k].reshape(ROWS, 16, lanes)
         for g in range(GROUPS):
             flat[16 * g : 16 * g + 16] = tiles[g]
-
-        @pl.when(k == SELF_CHUNK)
-        def _():
+        if k == SELF_CHUNK:
             ret[k, yc] = back[k, yc]
 
         spread(b_copy, k)
@@ -509,51 +548,97 @@
         rows = tiles_to_rows(ret[k].reshape(ROWS, 16, lanes), perm_ref[...], lanes)
         block = jnp.concatenate([jnp.concatenate(r, axis=1) for r in rows], axis=0)
         dims = (((0,), (0,)), ((), ()))
-        acc[...] += lax.dot_general(
+        part = lax.dot_general(
             mix[k, 0], block, dims, preferred_element_type=jnp.float32
         ) + lax.dot_general(mix[k, 1], block, dims, preferred_element_type=jnp.float32)
-
-    stages = ((arrive, 0), (forward, 1), (multiply, 2), (relay, 3), (finish, 4), (combine, 5))
-
-    def step(s, carry):
-        for stage, lag in stages:
-            if stage is forward:
-
-                @pl.when(s == 0)
-                def _():
-                    with jax.named_scope("mixer_relay"):
-                        mixer_relay()
-
-                @pl.when(s == 3)
-                def _():
-                    with jax.named_scope("mixer_finish"):
-                        mixer_finish()
-
-            @pl.when(jnp.logical_and(s >= lag, s < lag + CHUNKS))
-            def _(stage=stage, lag=lag):
-                with jax.named_scope(stage.__name__):
-                    stage(s - lag)
-
-        return carry
-
-    lax.fori_loop(0, CHUNKS + 5, step, 0)
-    out_ref[...] = acc[...].astype(jnp.bfloat16)
-
-    def drain(k, carry):
+        if k == last_combined:
+            out_ref[...] = (acc[...] + part).astype(jnp.bfloat16)
+            pltpu.make_async_copy(out_ref, moe_out, o_sem.at[1]).start()
+        elif k == first_combined:
+            acc[...] = part
+        else:
+            acc[...] += part
+
+    stages = dict(
+        D=dispatch,
+        B=begin,
+        S=send,
+        O=mixer_own,
+        H=mixer_halo,
+        P=mixer_transit,
+        Q=mixer_direct,
+        R=mixer_relay,
+        X=mixer_finish,
+        A=arrive,
+        F=forward,
+        W=multiply,
+        M=functools.partial(multiply, sends=False),
+        T=hand_on,
+        L=relay,
+        E=finish,
+        C=combine,
+    )
+    order = ORDER.split()
+    first_multiplied = [int(o[1]) for o in order if o[0] in "MW"][0]
+    combined = [int(o[1]) for o in order if o[0] == "C"]
+    first_combined, last_combined = combined[0], combined[-1]
+    for op in order:
+        with jax.named_scope(op):
+            stages[op[0]](*(int(k) for k in op[1:]))
+
+    def drain(k):
         bulk(outb, a_send, k)
         bulk(back, b_send, k)
         for which in range(4):
             g_copy(k, which).wait_send()
         for which in range(6):
             q_copy(k, which).wait_send()
-        return carry
 
     with jax.named_scope("drain"):
+        pltpu.make_async_copy(mixed_ref, mixed_out, o_sem.at[0]).wait()
+        pltpu.make_async_copy(out_ref, moe_out, o_sem.at[1]).wait()
         for which in range(2):
             h_copy(which).wait_send()
         for which in range(6):
             m_copy(which).wait_send()
-        lax.fori_loop(0, CHUNKS, drain, 0)
+        for k in range(CHUNKS):
+            drain(k)
+
+
+def settle_kernel(mixed_in, moe_in, mixed_out, moe_out, mixed_ref, moe_ref, in_sem, out_sem):
+    pieces = [(mixed_in, mixed_ref, mixed_out, 0)] + [
+        (moe_in, moe_ref, moe_out, SETTLE_ROWS * p) for p in range(moe_ref.shape[0] // SETTLE_ROWS)
+    ]
+    loads, stores = [], []
+    for n, (src, held, dst, first) in enumerate(pieces):
+        rows = pl.ds(first, SETTLE_ROWS)
+        loads.append(pltpu.make_async_copy(src.at[rows], held.at[rows], in_sem.at[n]))
+        stores.append(pltpu.make_async_copy(held.at[rows], dst.at[rows], out_sem.at[n]))
+    for load in loads:
+        load.start()
+    for load, store in zip(loads, stores):
+        load.wait()
+        store.start()
+    for store in stores:
+        store.wait()
+
+
+def settle(mixed, moe):
+    pieces = 1 + moe.shape[0] // SETTLE_ROWS
+    hbm = pl.BlockSpec(memory_space=pl.ANY)
+    return pl.pallas_call(
+        settle_kernel,
+        out_shape=tuple(jax.ShapeDtypeStruct(a.shape, a.dtype) for a in (mixed, moe)),
+        in_specs=[hbm, hbm],
+        out_specs=(hbm, hbm),
+        scratch_shapes=[
+            pltpu.VMEM(mixed.shape, mixed.dtype),
+            pltpu.VMEM(moe.shape, moe.dtype),
+            pltpu.SemaphoreType.DMA((pieces,)),
+            pltpu.SemaphoreType.DMA((pieces,)),
+        ],
+        compiler_params=pltpu.CompilerParams(vmem_limit_bytes=58 * 1024 * 1024),
+    )(mixed, moe)
 
 
 def shards(
@@ -577,20 +662,32 @@
     lanes = width // 16
     own_rows = queries.shape[0] // n_tp
     bf16 = jnp.bfloat16
-    vmem = pl.BlockSpec(memory_space=pltpu.VMEM)
-    smem = pl.BlockSpec(memory_space=pltpu.SMEM)
     hbm = pl.BlockSpec(memory_space=pl.ANY)
     dma = pltpu.SemaphoreType.DMA
     tiles = (CHUNKS, HALVES * N_YC, CAP, 16, lanes)
-    return pl.pallas_call(
+    small = (
+        moe_tokens,
+        moe_gain[None, :],
+        routes.T,
+        route_weights.T,
+        queries.T,
+        key_rows.T,
+        value_rows.T,
+        sink_logits[None, :],
+        mix_gain[None, :],
+    )
+    mixed, moe = pl.pallas_call(
         functools.partial(layer_kernel, n_tp),
         out_shape=(
             jax.ShapeDtypeStruct((own_rows, width), bf16),
             jax.ShapeDtypeStruct((tok, width), bf16),
         ),
-        in_specs=[vmem] * 7 + [smem, vmem] + [hbm] * 4,
-        out_specs=(vmem, vmem),
+        in_specs=[hbm] * 13,
+        out_specs=(hbm, hbm),
         scratch_shapes=[
+            *[pltpu.VMEM(a.shape, a.dtype) for a in small],
+            pltpu.VMEM((own_rows, width), bf16),
+            pltpu.VMEM((tok, width), bf16),
             pltpu.VMEM(tiles, bf16),
             pltpu.VMEM(tiles, bf16),
             pltpu.VMEM((CHUNKS, n_tp, ROWS, width), bf16),
@@ -612,6 +709,8 @@
             pltpu.VMEM((n_tp, own_rows, width), bf16),
             pltpu.VMEM((2, own_rows, width // 2), bf16),
             pltpu.VMEM((2, own_rows, width), bf16),
+            dma((len(small),)),
+            dma((2,)),
             dma((2,)),
             dma((2,)),
             dma((6,)),
@@ -629,21 +728,8 @@
         compiler_params=pltpu.CompilerParams(
             collective_id=0, has_side_effects=True, vmem_limit_bytes=58 * 1024 * 1024
         ),
-    )(
-        moe_tokens,
-        moe_gain[None, :],
-        routes.T,
-        route_weights.T,
-        queries.T,
-        key_rows.T,
-        value_rows.T,
-        sink_logits,
-        mix_gain[None, :],
-        expert_gate,
-        expert_up,
-        expert_down,
-        out_weight,
-    )
+    )(*small, expert_gate, expert_up, expert_down, out_weight)
+    return settle(mixed, moe)
 
 
 def solution(mesh):

time: 136 us -> 123 us (0.904)
  Pallas kernels: 132 us -> 122 us
  local copies, waits for them, and re-layouts: 3.55 us -> 0 us
    pallas_call x1, Pallas kernels: 132 us -> 120 us  [shards(): pl.pallas_call(functools.partial(layer_kernel, n_tp), out_shape=(jax.Shap...]
    unnamed x2 -> x0, local copies, waits for them, and re-layouts: 3.55 us -> none
    pallas_call x0 -> x1, Pallas kernels: none -> 1.88 us  [settle(): pl.pallas_call(settle_kernel, out_shape=tuple((jax.ShapeDtypeStruct(a.sha...]
where the time goes in v3:
time: 123 us; the launch traced here: 122 us
  Pallas kernels  122 us (99%)
    pallas_call x1, Pallas kernels, shards(): pl.pallas_call(functools.partial(layer_kernel, n_tp), out_shape=(jax.Shap...  120 us

profile of v3, /device:TPU:1, one launch (start us, length us, event | category | flops | bytes accessed | tf_op | source)
XLA Modules:
  0.0 122.4 jit_solution(11565809217971984939)
XLA Ops:
  0.6 119.7 %shard_map.140 = (bf16[64,2048]{1,0:T(8,128)(2,1)}, bf16[128,2048]{1,0:T(8,128)(2,1)}) custom-call(bf16[128,2048]{1,0:T(8,128)(2,1)} %tokens_in.1, f32[1,2048]{1,0:T(1,128)} %bitcast.11, s32[2,128]{1,0:T(2,128)} %bitcast.13, f32[2,128]{1,0:T(2,128)} %bitcast.14, bf16[192,256]{1,0:T(8,128)(2,1)} %bitcast.8, bf16[64,256]{1,0:T(8,128)(2,1)} %bitcast.9, ...), custom_call_target="tpu_custom_call" | custom-call | tf_op jit(solution)/shard_map/pallas_call | solution.py:679
  120.4 1.9 %shard_map.141 = (bf16[64,2048]{1,0:T(8,128)(2,1)}, bf16[128,2048]{1,0:T(8,128)(2,1)}) custom-call(bf16[64,2048]{1,0:T(8,128)(2,1)} %get-tuple-element.4.mixed_in, bf16[128,2048]{1,0:T(8,128)(2,1)} %get-tuple-element.5.moe_in), custom_call_target="tpu_custom_call" | custom-call | tf_op jit(solution)/shard_map/pallas_call | solution.py:629

commit v4 on v3

--- a/solution.py
+++ b/solution.py
@@ -20,11 +20,11 @@
 CHUNKS = 4
 HALVES = 2
 OFFSETS = ((2, 6), (4, 7), (3, 5), (0, 1))
-SETTLE_ROWS = 64
 SELF_CHUNK = 3
 ORDER = (
-    "D3 B S3 D0 S0 O D1 D2 H Q S1 A3 A0 S2 F3 A1 F0 M3 F1 A2 M0 W1 F2 L1 T0 M2 E1 L0 T2 E0 L2 T3 "
-    "C1 E2 L3 P C0 E3 R C2 X C3"
+    "D3", "B", "S3", "D0", "S0", "O", "D1", "D2", "H", "Q", "A3", "S1", "A0", "F3", "S2", "A1",
+    "F0", "M3", "F1", "A2", "W1", "M0", "F2", "L1", "T0", "M2", "E1", "L0", "T2", "E0", "L2", "T3",
+    "C1", "E2", "L3", "P", "C0", "E3", "R", "C2", "X", "C3",
 )
 ROWS = HALVES * N_YC * CAP
 GROUPS = ROWS // 16
@@ -72,8 +72,8 @@
     up_ref,
     down_ref,
     project_ref,
-    mixed_out,
-    moe_out,
+    mixed_ref,
+    out_ref,
     tokens_ref,
     gain_ref,
     routes_ref,
@@ -83,8 +83,6 @@
     values_ref,
     sink_ref,
     mix_gain_ref,
-    mixed_ref,
-    out_ref,
     outb,
     recv,
     xbuf,
@@ -107,7 +105,6 @@
     m1,
     m2,
     i_sem,
-    o_sem,
     h_send,
     h_recv,
     m_send,
@@ -153,15 +150,17 @@
     n_ep = N_Z * N_YC
 
     def greet(i, carry):
-        other = lax.rem(me + n_ep // 2 + i, jnp.int32(n_ep))
-
-        @pl.when(other != me)
+        ahead = lax.rem(me + n_ep // 2 + i, jnp.int32(n_ep))
+        behind = lax.rem(me + n_ep // 2 - 1 - i + n_ep, jnp.int32(n_ep))
+        pl.semaphore_signal(barrier, inc=1, device_id={"ep": ahead}, device_id_type=MESH)
+
+        @pl.when(behind != me)
         def _():
-            pl.semaphore_signal(barrier, inc=1, device_id={"ep": other}, device_id_type=MESH)
+            pl.semaphore_signal(barrier, inc=1, device_id={"ep": behind}, device_id_type=MESH)
 
         return carry
 
-    lax.fori_loop(0, n_ep, greet, 0)
+    lax.fori_loop(0, n_ep // 2, greet, 0)
     pl.semaphore_signal(barrier, inc=1, device_id={"tp": right}, device_id_type=MESH)
     pl.semaphore_signal(barrier, inc=1, device_id={"tp": left}, device_id_type=MESH)
 
@@ -238,9 +237,9 @@
         )
 
     def spread(copy_of, k):
-        def one(j, carry):
-            y = (yc + 1 + j) & (N_YC - 1)
-            for i in range(HALVES):
+        def one(j, carry, halves):
+            y = (yc + N_YC // 2 + j) & (N_YC - 1)
+            for i in halves:
                 if OFFSETS[k][i] == 0:
 
                     @pl.when(y != yc)
@@ -250,7 +249,8 @@
                     copy_of(k, i, y).start()
             return carry
 
-        lax.fori_loop(0, N_YC, one, 0)
+        for halves in ((1,), (0,)) if k == SELF_CHUNK else ((0, 1),):
+            lax.fori_loop(0, N_YC, functools.partial(one, halves=halves), 0)
 
     def bulk(buffer, sem, k):
         count = HALVES * N_YC - (k == SELF_CHUNK)
@@ -418,7 +418,6 @@
         mixed_ref[...] = (total * lax.rsqrt(squares + norm_eps) * mix_gain_ref[...]).astype(
             jnp.bfloat16
         )
-        pltpu.make_async_copy(mixed_ref, mixed_out, o_sem.at[0]).start()
 
     low = pl.ds(0, half)
     high = pl.ds(half, half)
@@ -553,7 +552,6 @@
         ) + lax.dot_general(mix[k, 1], block, dims, preferred_element_type=jnp.float32)
         if k == last_combined:
             out_ref[...] = (acc[...] + part).astype(jnp.bfloat16)
-            pltpu.make_async_copy(out_ref, moe_out, o_sem.at[1]).start()
         elif k == first_combined:
             acc[...] = part
         else:
@@ -578,7 +576,7 @@
         E=finish,
         C=combine,
     )
-    order = ORDER.split()
+    order = ORDER
     first_multiplied = [int(o[1]) for o in order if o[0] in "MW"][0]
     combined = [int(o[1]) for o in order if o[0] == "C"]
     first_combined, last_combined = combined[0], combined[-1]
@@ -595,8 +593,6 @@
             q_copy(k, which).wait_send()
 
     with jax.named_scope("drain"):
-        pltpu.make_async_copy(mixed_ref, mixed_out, o_sem.at[0]).wait()
-        pltpu.make_async_copy(out_ref, moe_out, o_sem.at[1]).wait()
         for which in range(2):
             h_copy(which).wait_send()
         for which in range(6):
@@ -605,40 +601,28 @@
             drain(k)
 
 
-def settle_kernel(mixed_in, moe_in, mixed_out, moe_out, mixed_ref, moe_ref, in_sem, out_sem):
-    pieces = [(mixed_in, mixed_ref, mixed_out, 0)] + [
-        (moe_in, moe_ref, moe_out, SETTLE_ROWS * p) for p in range(moe_ref.shape[0] // SETTLE_ROWS)
+def settle_kernel(mixed_ref, moe_ref, mixed_out, moe_out, sem):
+    copies = [
+        pltpu.make_async_copy(mixed_ref, mixed_out, sem.at[0]),
+        pltpu.make_async_copy(moe_ref, moe_out, sem.at[1]),
     ]
-    loads, stores = [], []
-    for n, (src, held, dst, first) in enumerate(pieces):
-        rows = pl.ds(first, SETTLE_ROWS)
-        loads.append(pltpu.make_async_copy(src.at[rows], held.at[rows], in_sem.at[n]))
-        stores.append(pltpu.make_async_copy(held.at[rows], dst.at[rows], out_sem.at[n]))
-    for load in loads:
-        load.start()
-    for load, store in zip(loads, stores):
-        load.wait()
-        store.start()
-    for store in stores:
-        store.wait()
+    for copy in copies:
+        copy.start()
+    for copy in copies:
+        copy.wait()
 
 
 def settle(mixed, moe):
-    pieces = 1 + moe.shape[0] // SETTLE_ROWS
     hbm = pl.BlockSpec(memory_space=pl.ANY)
+    vmem = pl.BlockSpec(memory_space=pltpu.VMEM)
     return pl.pallas_call(
         settle_kernel,
         out_shape=tuple(jax.ShapeDtypeStruct(a.shape, a.dtype) for a in (mixed, moe)),
-        in_specs=[hbm, hbm],
+        in_specs=[vmem, vmem],
         out_specs=(hbm, hbm),
-        scratch_shapes=[
-            pltpu.VMEM(mixed.shape, mixed.dtype),
-            pltpu.VMEM(moe.shape, moe.dtype),
-            pltpu.SemaphoreType.DMA((pieces,)),
-            pltpu.SemaphoreType.DMA((pieces,)),
-        ],
+        scratch_shapes=[pltpu.SemaphoreType.DMA((2,))],
         compiler_params=pltpu.CompilerParams(vmem_limit_bytes=58 * 1024 * 1024),
-    )(mixed, moe)
+    )(*(pltpu.with_memory_space_constraint(a, pltpu.VMEM) for a in (mixed, moe)))
 
 
 def shards(
@@ -663,6 +647,7 @@
     own_rows = queries.shape[0] // n_tp
     bf16 = jnp.bfloat16
     hbm = pl.BlockSpec(memory_space=pl.ANY)
+    vmem = pl.BlockSpec(memory_space=pltpu.VMEM)
     dma = pltpu.SemaphoreType.DMA
     tiles = (CHUNKS, HALVES * N_YC, CAP, 16, lanes)
     small = (
@@ -678,16 +663,11 @@
     )
     mixed, moe = pl.pallas_call(
         functools.partial(layer_kernel, n_tp),
-        out_shape=(
-            jax.ShapeDtypeStruct((own_rows, width), bf16),
-            jax.ShapeDtypeStruct((tok, width), bf16),
-        ),
+        out_shape=(pltpu.VMEM((own_rows, width), bf16), pltpu.VMEM((tok, width), bf16)),
         in_specs=[hbm] * 13,
-        out_specs=(hbm, hbm),
+        out_specs=(vmem, vmem),
         scratch_shapes=[
             *[pltpu.VMEM(a.shape, a.dtype) for a in small],
-            pltpu.VMEM((own_rows, width), bf16),
-            pltpu.VMEM((tok, width), bf16),
             pltpu.VMEM(tiles, bf16),
             pltpu.VMEM(tiles, bf16),
             pltpu.VMEM((CHUNKS, n_tp, ROWS, width), bf16),
@@ -712,7 +692,6 @@
             dma((len(small),)),
             dma((2,)),
             dma((2,)),
-            dma((2,)),
             dma((6,)),
             dma((6,)),
             dma((3,)),

time: 123 us -> 119 us (0.967)
  Pallas kernels: 122 us -> 118 us
    pallas_call x1, Pallas kernels: 120 us -> 117 us  [shards(): pl.pallas_call(functools.partial(layer_kernel, n_tp), out_shape=(pltpu.VM...]
where the time goes in v4:
time: 119 us; the launch traced here: 118 us
  Pallas kernels  118 us (99%)
    pallas_call x1, Pallas kernels, shards(): pl.pallas_call(functools.partial(layer_kernel, n_tp), out_shape=(pltpu.VM...  117 us

profile of v4, /device:TPU:1, one launch (start us, length us, event | category | flops | bytes accessed | tf_op | source)
XLA Modules:
  0.0 118.4 jit_solution(13001285622227175784)
XLA Ops:
  0.6 116.7 %shard_map.140 = (bf16[64,2048]{1,0:T(8,128)(2,1)S(1)}, bf16[128,2048]{1,0:T(8,128)(2,1)S(1)}) custom-call(bf16[128,2048]{1,0:T(8,128)(2,1)} %tokens_in.1, f32[1,2048]{1,0:T(1,128)} %bitcast.11, s32[2,128]{1,0:T(2,128)} %bitcast.13, f32[2,128]{1,0:T(2,128)} %bitcast.14, bf16[192,256]{1,0:T(8,128)(2,1)} %bitcast.8, bf16[64,256]{1,0:T(8,128)(2,1)} %bitcast.9, ...), custom_call_target="tpu_custom_call" | custom-call | tf_op jit(solution)/shard_map/pallas_call | solution.py:664
  117.4 0.9 shard_map.141

commit v5 on v4

--- a/solution.py
+++ b/solution.py
@@ -19,12 +19,12 @@
 CAP = 5
 CHUNKS = 4
 HALVES = 2
-OFFSETS = ((2, 6), (4, 7), (3, 5), (0, 1))
+OFFSETS = ((2, 6), (3, 5), (4, 7), (0, 1))
 SELF_CHUNK = 3
 ORDER = (
-    "D3", "B", "S3", "D0", "S0", "O", "D1", "D2", "H", "Q", "A3", "S1", "A0", "F3", "S2", "A1",
+    "D3", "B", "S3", "D0", "S0", "O", "H", "P", "D1", "D2", "A3", "S1", "A0", "F3", "S2", "A1",
     "F0", "M3", "F1", "A2", "W1", "M0", "F2", "L1", "T0", "M2", "E1", "L0", "T2", "E0", "L2", "T3",
-    "C1", "E2", "L3", "P", "C0", "E3", "R", "C2", "X", "C3",
+    "C1", "E2", "L3", "R", "Q", "C0", "E3", "C2", "X", "C3",
 )
 ROWS = HALVES * N_YC * CAP
 GROUPS = ROWS // 16

time: 119 us -> 118 us (level)
  no operation moved by 1% of the time
where the time goes in v5:
time: 118 us
  Pallas kernels  117 us (99%)
    pallas_call x1, Pallas kernels, shards(): pl.pallas_call(functools.partial(layer_kernel, n_tp), out_shape=(pltpu.VM...  116 us

profile of v5, /device:TPU:1, one launch (start us, length us, event | category | flops | bytes accessed | tf_op | source)
XLA Modules:
  0.0 118.1 jit_solution(15802555097199888363)
XLA Ops:
  0.6 116.3 %shard_map.140 = (bf16[64,2048]{1,0:T(8,128)(2,1)S(1)}, bf16[128,2048]{1,0:T(8,128)(2,1)S(1)}) custom-call(bf16[128,2048]{1,0:T(8,128)(2,1)} %tokens_in.1, f32[1,2048]{1,0:T(1,128)} %bitcast.11, s32[2,128]{1,0:T(2,128)} %bitcast.13, f32[2,128]{1,0:T(2,128)} %bitcast.14, bf16[192,256]{1,0:T(8,128)(2,1)} %bitcast.8, bf16[64,256]{1,0:T(8,128)(2,1)} %bitcast.9, ...), custom_call_target="tpu_custom_call" | custom-call | tf_op jit(solution)/shard_map/pallas_call | solution.py:664
  117.0 0.9 shard_map.141

commit v6 on v5

--- a/solution.py
+++ b/solution.py
@@ -22,7 +22,7 @@
 OFFSETS = ((2, 6), (3, 5), (4, 7), (0, 1))
 SELF_CHUNK = 3
 ORDER = (
-    "D3", "B", "S3", "D0", "S0", "O", "H", "P", "D1", "D2", "A3", "S1", "A0", "F3", "S2", "A1",
+    "D3", "D0", "B", "S3", "S0", "O", "H", "P", "D1", "D2", "A3", "S1", "A0", "F3", "S2", "A1",
     "F0", "M3", "F1", "A2", "W1", "M0", "F2", "L1", "T0", "M2", "E1", "L0", "T2", "E0", "L2", "T3",
     "C1", "E2", "L3", "R", "Q", "C0", "E3", "C2", "X", "C3",
 )

time: 118 us -> 118 us (level)
  no operation moved by 1% of the time
where the time goes in v6:
time: 118 us
  Pallas kernels  117 us (99%)
    pallas_call x1, Pallas kernels, shards(): pl.pallas_call(functools.partial(layer_kernel, n_tp), out_shape=(pltpu.VM...  117 us

profile of v6, /device:TPU:1, one launch (start us, length us, event | category | flops | bytes accessed | tf_op | source)
XLA Modules:
  0.0 118.3 jit_solution(7537817663507307069)
XLA Ops:
  0.6 116.6 %shard_map.140 = (bf16[64,2048]{1,0:T(8,128)(2,1)S(1)}, bf16[128,2048]{1,0:T(8,128)(2,1)S(1)}) custom-call(bf16[128,2048]{1,0:T(8,128)(2,1)} %tokens_in.1, f32[1,2048]{1,0:T(1,128)} %bitcast.11, s32[2,128]{1,0:T(2,128)} %bitcast.13, f32[2,128]{1,0:T(2,128)} %bitcast.14, bf16[192,256]{1,0:T(8,128)(2,1)} %bitcast.8, bf16[64,256]{1,0:T(8,128)(2,1)} %bitcast.9, ...), custom_call_target="tpu_custom_call" | custom-call | tf_op jit(solution)/shard_map/pallas_call | solution.py:664
  117.2 0.9 shard_map.141
